TPU v7x, 256 devices: a whole 4x4x8 slice. The times are simulated.
256 devices in a mesh: sp: 64 (over z, y, core), tp: 4 (over x).
Axes of the slice: x: 4, y: 4, z: 8, core: 2. Of those that a mesh axis runs over, the one named last changes fastest.
Arguments:
- stream: bfloat16 [65536, 4096], P('sp', 'tp'), may hold values from -11 to 11
- norm_gain: bfloat16 [3, 4096], P(None, 'tp'), may hold values from 0.099609375 to 1.8984375
- pool_weight: bfloat16 [3, 4, 1024, 1024], P(None, 'tp', 'sp'), may hold values from -0.1875 to 0.1875
- pool_scale: bfloat16 [3, 4096], P(None, 'tp'), may hold values from 0.099609375 to 1.8984375
Outputs:
- mixed: bfloat16 [65536, 4096], P('sp', 'tp')
All inputs are finite; a program needn't handle non-finite values.
Results may differ from a plain program's by a relative error of at most 0.015.
Values may be sent and summed in bfloat16 or wider, within the bound.
No kernel may reach another device: no remote copies, remote signals or barrier semaphores. Data moves between devices by JAX's collectives and lax.ppermute only.
A program may use at most 64 MiB of HBM per device.

v0:
```python
import functools

import jax
import jax.numpy as jnp
from jax import lax
from jax.experimental import pallas as pl
from jax.experimental.pallas import tpu as pltpu
from jax.sharding import PartitionSpec as P


D = 4096
EPS = 1e-06
HALO = 32
Z, Y, C = 8, 4, 2
VMEM = pl.BlockSpec(memory_space=pltpu.VMEM)


def split(sp):
    return sp // (Y * C), (sp // C) % Y, sp % C


def join(z, y, c):
    return ((z % Z) * Y + y % Y) * C + c


def toward(i, c):
    return 1 - 2 * ((i + c) % 2)


def trade(value, axis, step):
    found = []
    for sp in range(Z * Y * C):
        z, y, c = split(sp)
        sign = (2, 1, -1)[step]
        if axis == "z":
            to = join(z + sign * toward(z, c), y, c)
        else:
            to = join(z, y + sign * toward(y, c), c)
        found.append((sp, to))
    return lax.ppermute(value, "sp", found)


def partner(value):
    return lax.ppermute(value, "sp", [(sp, sp ^ 1) for sp in range(Z * Y * C)])


RING4 = (0, 1, -1, -2)
RING8 = (0, 1, -1, -2, 2, 3, -3, -4)


def after(value, other):
    return lax.optimization_barrier((value, other))[0]


def pack(parts, lo, hi):
    def kernel(*refs):
        out, at = refs[-1], 0
        for ref in refs[:-1]:
            n = ref.shape[0]
            out[at : at + n] = ref[:, lo:hi]
            at += n

    slots, _, *tail = parts[0].shape
    slots = sum(p.shape[0] for p in parts)
    return pl.pallas_call(
        kernel,
        out_shape=jax.ShapeDtypeStruct((slots, hi - lo, *tail), parts[0].dtype),
        in_specs=[VMEM] * len(parts),
        out_specs=VMEM,
        compiler_params=pltpu.CompilerParams(vmem_limit_bytes=2**23),
        name="pack",
    )(*parts)


def slots(zs, ys):
    return [(z, y) for z in zs for y in ys]


def gather(own, fetched):
    layers = own.shape[1]
    beside = [trade(own, "y", 1), trade(own, "y", 2), trade(own, "y", 0)]
    behind = trade(own, "z", 1)

    line = pack((fetched, *beside), 0, 1)
    near = pack((line, trade(line, "z", 1)), 0, 1)
    second = trade(near, "z", 2)
    third = trade(second, "z", 1)
    fourth = trade(third, "z", 2)
    here = slots(RING8[:4], RING4)
    inner = pack((near, second), 0, 1)
    early = partner(inner)
    outer = pack((third, fourth), 0, 1)
    there = slots(RING8[4:], RING4)
    out = [[(inner, here, 0), (early, here, 1), (outer, there, 0), (partner(outer), there, 1)]]

    two = pack((fetched, behind), 1, layers)
    second = trade(two, "z", 2)
    third = trade(second, "z", 1)
    line = pack((two, second, third, after(trade(third, "z", 2), early)), 0, layers - 1)
    beside = after(trade(line, "y", 1), fourth)
    for i in range(layers - 1):
        near = pack((line, beside), i, i + 1)
        far = trade(near, "y", 2)
        out.append((near, far))
    return out, early


def finish(near, far, other):
    piece = pack((near, after(far, other)), 0, 1)
    where = [(z, y) for y in RING4 for z in RING8]
    return [(piece, where, 0), (partner(piece), where, 1)]


def squares(x):
    rows = x.shape[0]
    lane = lax.broadcasted_iota(jnp.int32, (128, 128), 1)
    cols = jnp.zeros((128, 128), jnp.float32)
    for i in range(0, rows, 128):
        n = min(128, rows - i)
        part = x[i : i + n]
        if n < 128:
            part = jnp.concatenate([part, jnp.zeros((128 - n, part.shape[1]), jnp.float32)])
        cols = jnp.where(lane == i // 128, jnp.sum(part, axis=1, keepdims=True), cols)
    return cols.T[:16]


def prepare_kernel(own, x, kept, within, across, edge, arrived):
    rows = x.shape[0]
    copies = [
        pltpu.make_async_copy(x.at[pl.ds(0, HALO)], edge.at[0], arrived.at[0]),
        pltpu.make_async_copy(x.at[pl.ds(rows - HALO, HALO)], edge.at[1], arrived.at[1]),
        pltpu.make_async_copy(own, kept, arrived.at[2]),
    ]
    for copy in copies:
        copy.start()
    even = lax.rem(lax.axis_index("sp"), 2) == 0
    for copy in copies[:2]:
        copy.wait()
    within[...] = jnp.where(even, edge[1], edge[0])
    across[...] = jnp.where(even, edge[0], edge[1])
    copies[2].wait()


def add_kernel(a, b, out):
    out[...] = a[...] + b[...]


def first_kernel(within, across, x, ext, sums, arrived):
    rows = x.shape[0]
    total = ext.shape[0]
    part = rows // 4
    copies = [
        pltpu.make_async_copy(
            x.at[pl.ds(i * part, part)], ext.at[pl.ds(HALO + i * part, part)], arrived.at[i]
        )
        for i in range(4)
    ]
    for copy in copies:
        copy.start()
    even = lax.rem(lax.axis_index("sp"), 2) == 0
    ext[:HALO] = jnp.where(even, across[...], within[...])
    ext[HALO + rows :] = jnp.where(even, within[...], across[...])
    acc = []
    edges = (0, HALO + part, HALO + 2 * part, HALO + 3 * part, total)
    for i, (lo, hi) in enumerate(zip(edges, edges[1:])):
        copies[i].wait()
        found = jnp.zeros((hi - lo, 128), jnp.float32)
        for j in range(0, x.shape[1], 128):
            v = ext[lo:hi, j : j + 128].astype(jnp.float32)
            found += v * v
        acc.append(found)
    sums[...] = squares(jnp.concatenate(acc))


def map_kernel(layer, places, x_ref, gain_ref, *refs):
    pieces, (out_ref, w) = refs[: len(places)], refs[len(places) :]
    total, width = x_ref.shape
    sp = lax.axis_index("sp")
    z, y, c = sp // (Y * C), lax.rem(sp // C, Y), lax.rem(sp, C)

    for ref, (where, other) in zip(pieces, places, strict=True):
        core = 1 - c if other else c
        dz, dy = 1 - 2 * lax.rem(z + core, 2), 1 - 2 * lax.rem(y + core, 2)
        for j, (fz, fy) in enumerate(where):
            at = (lax.rem(z + fz * dz + Z, Z) * Y + lax.rem(y + fy * dy + Y, Y)) * C + core
            w[pl.ds(pl.multiple_of(at * 16, 16), 16), :] = ref[j, 0]

    gain = gain_ref[layer : layer + 1, :].astype(jnp.float32)
    step = 272
    for i in range(0, total, step):
        scaled = (x_ref[i : i + step].astype(jnp.float32) * gain).astype(jnp.bfloat16)
        for j in range(0, width, 256):
            out_ref[i : i + step, j : j + 256] = jnp.dot(
                scaled, w[:, j : j + 256], preferred_element_type=jnp.float32
            )


def pool_kernel(layer, lo, hi, last, tokens, n_parts, *refs):
    x_ref, mapped_ref, scale_ref, *refs = refs
    parts, refs = refs[:n_parts], refs[n_parts:]
    if last:
        out_ref, normed, held, sent = refs
    else:
        out_ref, sums_ref, normed, acc = refs
    total, width = x_ref.shape
    scale_of = lax.rsqrt(sum(p[...] for p in parts) / D + EPS)
    column = jnp.concatenate([scale_of, jnp.zeros((112, 128), jnp.float32)]).T
    for i in range(0, total, 128):
        m = min(128, total - i)
        r = column[:m, i // 128 : i // 128 + 1]
        normed[i : i + m] = (mapped_ref[i : i + m] * r).astype(jnp.bfloat16)

    first = lax.axis_index("sp") * (total - 2 * HALO) - HALO
    half = jnp.left_shift(jnp.int32(1), lax.axis_index("tp"))
    scale = scale_ref[layer : layer + 1, :].astype(jnp.float32)
    if not last:
        acc[:lo] = jnp.zeros((lo, 128), jnp.float32)
        acc[hi:] = jnp.zeros((total - hi, 128), jnp.float32)
        out_ref[:lo] = x_ref[:lo]
        out_ref[hi:] = x_ref[hi:]
    step = 224
    copies = []
    for b in range(lo, hi, step):
        m = min(step, hi - b)
        k = m + 32
        t = first + b + lax.broadcasted_iota(jnp.int32, (m, k), 0)
        s = first + b - 16 + lax.broadcasted_iota(jnp.int32, (m, k), 1)
        inside = (s >= jnp.maximum(t - half, 0)) & (s < jnp.minimum(t + half, tokens))
        count = jnp.maximum(jnp.minimum(t + half, tokens) - jnp.maximum(t - half, 0), 1)
        band = jnp.where(inside, 1.0 / count.astype(jnp.float32), 0.0) - (s == t).astype(jnp.float32)
        band = band.astype(jnp.bfloat16)
        squared = None
        for j in range(0, width, 256):
            branch = jnp.dot(band, normed[b - 16 : b - 16 + k, j : j + 256], preferred_element_type=jnp.float32)
            new = x_ref[b : b + m, j : j + 256].astype(jnp.float32) + branch * scale[:, j : j + 256]
            new = new.astype(jnp.bfloat16)
            if last:
                held[b - lo : b - lo + m, j : j + 256] = new
            else:
                out_ref[b : b + m, j : j + 256] = new
                new = new.astype(jnp.float32)
                new = new * new
                new = new[:, :128] + new[:, 128:]
                squared = new if squared is None else squared + new
        if last:
            rows = pl.ds(b - lo, m)
            copies.append(pltpu.make_async_copy(held.at[rows], out_ref.at[rows], sent.at[len(copies)]))
            copies[-1].start()
        else:
            acc[b : b + m] = squared
    if not last:
        sums_ref[...] = squares(acc[...])
    for copy in copies:
        copy.wait()


def over_tp(sums):
    n = lax.axis_size("tp")
    found = [sums]
    for k in (1, 3, 2):
        found.append(lax.ppermute(sums, "tp", [(i, i ^ k) for i in range(n)]))
    return found


def program(stream, norm_gain, pool_weight, pool_scale):
    rows, width = stream.shape
    layers, _, shard, _ = pool_weight.shape
    devices = lax.axis_size("sp")
    total = rows + 2 * HALO
    own = pool_weight.reshape(1, layers, shard, width)
    edge = jax.ShapeDtypeStruct((HALO, width), stream.dtype)
    fetched, within, across = pl.pallas_call(
        prepare_kernel,
        out_shape=(jax.ShapeDtypeStruct(own.shape, own.dtype), edge, edge),
        in_specs=[pl.BlockSpec(memory_space=pltpu.HBM)] * 2,
        out_specs=(VMEM,) * 3,
        scratch_shapes=[pltpu.VMEM((2, HALO, width), stream.dtype), pltpu.SemaphoreType.DMA((3,))],
        compiler_params=pltpu.CompilerParams(vmem_limit_bytes=125 * 2**19),
        name="prepare",
    )(own, stream)
    within = lax.ppermute(within, "sp", [(i, i ^ 1) for i in range(devices)])
    pairs = [(i, i + 1) for i in range(1, devices - 1, 2)]
    across = lax.ppermute(across, "sp", pairs + [(j, i) for i, j in pairs])
    params = pltpu.CompilerParams(vmem_limit_bytes=32 * 2**20)
    sums_type = jax.ShapeDtypeStruct((16, 128), jnp.float32)
    ext_type = jax.ShapeDtypeStruct((total, width), jnp.bfloat16)
    ext, sums = pl.pallas_call(
        first_kernel,
        out_shape=(ext_type, sums_type),
        in_specs=[VMEM, VMEM, pl.BlockSpec(memory_space=pltpu.HBM)],
        out_specs=(VMEM, VMEM),
        scratch_shapes=[pltpu.SemaphoreType.DMA((4,))],
        compiler_params=params,
        name="first",
    )(within, across, stream)
    other = lax.ppermute(sums, "tp", [(i, i ^ 1) for i in range(lax.axis_size("tp"))])
    gathered, early = gather(own, fetched)
    other = after(other, early)
    sums = pl.pallas_call(
        add_kernel, out_shape=sums_type, in_specs=[VMEM] * 2, out_specs=VMEM,
        compiler_params=pltpu.CompilerParams(vmem_limit_bytes=2**20), name="add",
    )(sums, other)
    other = lax.ppermute(sums, "tp", [(i, i ^ 3) for i in range(lax.axis_size("tp"))])
    traded = [sums, other]
    for layer in range(layers):
        pieces = finish(*gathered[layer], sums) if layer else gathered[0]
        last = layer == layers - 1
        lo, hi = (HALO, HALO + rows) if last else (16, total - 16)
        mapped = pl.pallas_call(
            functools.partial(map_kernel, layer, [p[1:] for p in pieces]),
            out_shape=jax.ShapeDtypeStruct((total, width), jnp.float32),
            in_specs=[VMEM] * (2 + len(pieces)),
            out_specs=VMEM,
            scratch_shapes=[pltpu.VMEM((width, width), jnp.bfloat16)],
            compiler_params=params,
            cost_estimate=pl.CostEstimate(
                flops=2 * total * width * width, bytes_accessed=6 * total * width, transcendentals=0
            ),
        )(ext, norm_gain, *[p[0] for p in pieces])
        scratch = [pltpu.VMEM((total, width), jnp.bfloat16)]
        if last:
            scratch += [pltpu.VMEM((rows, width), jnp.bfloat16), pltpu.SemaphoreType.DMA((5,))]
        else:
            scratch.append(pltpu.VMEM((total, 128), jnp.float32))
        out = pl.pallas_call(
            functools.partial(pool_kernel, layer, lo, hi, last, rows * devices, len(traded)),
            out_shape=jax.ShapeDtypeStruct((rows, width), jnp.bfloat16) if last else (ext_type, sums_type),
            in_specs=[VMEM] * (3 + len(traded)),
            out_specs=pl.BlockSpec(memory_space=pltpu.HBM) if last else (VMEM, VMEM),
            scratch_shapes=scratch,
            compiler_params=params,
            cost_estimate=pl.CostEstimate(
                flops=total * width * 512, bytes_accessed=8 * total * width, transcendentals=0
            ),
        )(ext, mapped, pool_scale, *traded)
        if not last:
            ext, sums = out
            traded = over_tp(sums)
    return out


def solution(mesh):
    placed = (P("sp", "tp"), P(None, "tp"), P(None, "tp", "sp", None), P(None, "tp"))
    return jax.shard_map(program, mesh=mesh, in_specs=placed, out_specs=P("sp", "tp"), check_vma=False)
```

profile of v0, /device:TPU:1, one launch (start us, length us, event | category | flops | bytes accessed | tf_op | source)
XLA Modules:
  0.0 103.1 jit_solution(13864339449814045755)
XLA Ops:
  0.0 3.6 %collective-permute-start.2 = (bf16[1,3,16,1024]{3,2,1,0:T(8,128)(2,1)}, bf16[1,3,16,1024]{3,2,1,0:T(8,128)(2,1)S(1)}, u32[]{:S(2)}, u32[]{:S(2)}) collective-permute-start(bf16[1,3,16,1024]{3,2,1,0:T(8,128)(2,1)} %bitcast.1), channel_id=1, source_target_pairs={{0,8},{4,28},{8,0},{12,20},{16,24},{20,12},{24,16},{28,4},{32,40},... | collective-permute-start | bytes 294920 | tf_op jit(solution)/shard_map/ppermute | solution.py:40
  3.6 0.0 collective-permute-start.3
  3.6 1.3 %collective-permute-start.4 = (bf16[1,3,16,1024]{3,2,1,0:T(8,128)(2,1)}, bf16[1,3,16,1024]{3,2,1,0:T(8,128)(2,1)S(1)}, u32[]{:S(2)}, u32[]{:S(2)}) collective-permute-start(bf16[1,3,16,1024]{3,2,1,0:T(8,128)(2,1)} %bitcast.3), channel_id=1, source_target_pairs={{0,16},{4,20},{8,24},{12,28},{16,0},{20,4},{24,8},{28,12},{32,48},... | collective-permute-start | bytes 294920 | tf_op jit(solution)/shard_map/ppermute | solution.py:40
  4.8 1.7 %prepare.1 = (bf16[1,3,16,1024]{3,2,1,0:T(8,128)(2,1)}, bf16[32,1024]{1,0:T(8,128)(2,1)}, bf16[32,1024]{1,0:T(8,128)(2,1)}) custom-call(bf16[1,3,16,1024]{3,2,1,0:T(8,128)(2,1)} %bitcast.4, bf16[1024,1024]{1,0:T(8,128)(2,1)} %x.3), custom_call_target="tpu_custom_call" | custom-call | tf_op jit(solution)/shard_map/prepare/pallas_call | solution.py:272
  6.5 0.0 collective-permute-done.2.refs_1_
  6.5 2.0 %collective-permute-done.3.refs_2_ = bf16[1,3,16,1024]{3,2,1,0:T(8,128)(2,1)S(1)} collective-permute-done((bf16[1,3,16,1024]{3,2,1,0:T(8,128)(2,1)}, bf16[1,3,16,1024]{3,2,1,0:T(8,128)(2,1)S(1)}, u32[]{:S(2)}, u32[]{:S(2)}) %collective-permute-start.3) | collective-permute-done | bytes 98336 | tf_op jit(solution)/shard_map/ppermute | solution.py:40
  8.5 0.8 collective-permute-done.4.refs_3_
  9.2 0.9 copy-done.1
  10.1 5.7 %collective-permute-start.5 = (bf16[4,1,16,1024]{3,2,1,0:T(8,128)(2,1)S(1)}, bf16[4,1,16,1024]{3,2,1,0:T(8,128)(2,1)S(1)}, u32[]{:S(2)}, u32[]{:S(2)}) collective-permute-start(bf16[4,1,16,1024]{3,2,1,0:T(8,128)(2,1)S(1)} %pack.10.refs_0_), channel_id=1, source_target_pairs={{0,32},{4,228},{8,40},{12,236},{16,48},{20,244},{24,56},{28,252},{... | collective-permute-start | bytes 393224 | tf_op jit(solution)/shard_map/ppermute | solution.py:40
  15.8 2.4 %collective-permute-done.5.refs_1_ = bf16[4,1,16,1024]{3,2,1,0:T(8,128)(2,1)S(1)} collective-permute-done((bf16[4,1,16,1024]{3,2,1,0:T(8,128)(2,1)S(1)}, bf16[4,1,16,1024]{3,2,1,0:T(8,128)(2,1)S(1)}, u32[]{:S(2)}, u32[]{:S(2)}) %collective-permute-start.5) | collective-permute-done | bytes 131104 | tf_op jit(solution)/shard_map/ppermute | solution.py:40
  18.2 0.1 collective-permute-start.6
  18.3 5.2 %collective-permute-done.6.refs_1_ = bf16[8,1,16,1024]{3,2,1,0:T(8,128)(2,1)S(1)} collective-permute-done((bf16[8,1,16,1024]{3,2,1,0:T(8,128)(2,1)S(1)}, bf16[8,1,16,1024]{3,2,1,0:T(8,128)(2,1)S(1)}, u32[]{:S(2)}, u32[]{:S(2)}) %collective-permute-start.6) | collective-permute-done | bytes 262176 | tf_op jit(solution)/shard_map/ppermute | solution.py:40
  23.6 0.0 copy-start
  23.6 4.4 %collective-permute-start.7 = (bf16[16,1,16,1024]{3,2,1,0:T(8,128)(2,1)S(1)}, bf16[16,1,16,1024]{3,2,1,0:T(8,128)(2,1)S(1)}, u32[]{:S(2)}, u32[]{:S(2)}) collective-permute-start(bf16[16,1,16,1024]{3,2,1,0:T(8,128)(2,1)S(1)} %pack.12.refs_0_), channel_id=1, source_target_pairs={{0,4},{4,0},{8,12},{12,8},{16,20},{20,16},{24,28},{28,24},{32,36},... | collective-permute-start | bytes 1572872 | tf_op jit(solution)/shard_map/ppermute | solution.py:44
  28.0 3.0 %collective-permute-start.13 = (bf16[1,3,16,1024]{3,2,1,0:T(8,128)(2,1)S(1)}, bf16[1,3,16,1024]{3,2,1,0:T(8,128)(2,1)S(1)}, u32[]{:S(2)}, u32[]{:S(2)}) collective-permute-start(bf16[1,3,16,1024]{3,2,1,0:T(8,128)(2,1)S(1)} %bitcast.5), channel_id=1, source_target_pairs={{0,32},{4,228},{8,40},{12,236},{16,48},{20,244},{24,56},{28,252},{... | collective-permute-start | bytes 294920 | tf_op jit(solution)/shard_map/ppermute | solution.py:40
  31.0 2.0 %collective-permute-done.13.refs_1_ = bf16[1,3,16,1024]{3,2,1,0:T(8,128)(2,1)S(1)} collective-permute-done((bf16[1,3,16,1024]{3,2,1,0:T(8,128)(2,1)S(1)}, bf16[1,3,16,1024]{3,2,1,0:T(8,128)(2,1)S(1)}, u32[]{:S(2)}, u32[]{:S(2)}) %collective-permute-start.13) | collective-permute-done | bytes 98336 | tf_op jit(solution)/shard_map/ppermute | solution.py:40
  33.0 0.1 collective-permute-start.14
  33.1 2.8 %collective-permute-start.8 = (bf16[8,1,16,1024]{3,2,1,0:T(8,128)(2,1)S(1)}, bf16[8,1,16,1024]{3,2,1,0:T(8,128)(2,1)S(1)}, u32[]{:S(2)}, u32[]{:S(2)}) collective-permute-start(bf16[8,1,16,1024]{3,2,1,0:T(8,128)(2,1)S(1)} %collective-permute-done.6.refs_1_), channel_id=1, source_target_pairs={{0,32},{4,228},{8,40},{12,236},{16,48},{20,244},{24,56},{28,252},{... | collective-permute-start | bytes 786440 | tf_op jit(solution)/shard_map/ppermute | solution.py:40
  35.9 1.0 %collective-permute-done.14.refs_1_ = bf16[2,2,16,1024]{3,2,1,0:T(8,128)(2,1)S(1)} collective-permute-done((bf16[2,2,16,1024]{3,2,1,0:T(8,128)(2,1)S(1)}, bf16[2,2,16,1024]{3,2,1,0:T(8,128)(2,1)S(1)}, u32[]{:S(2)}, u32[]{:S(2)}) %collective-permute-start.14) | collective-permute-done | bytes 131104 | tf_op jit(solution)/shard_map/ppermute | solution.py:40
  36.9 3.8 %collective-permute-start.15 = (bf16[2,2,16,1024]{3,2,1,0:T(8,128)(2,1)S(1)}, bf16[2,2,16,1024]{3,2,1,0:T(8,128)(2,1)S(1)}, u32[]{:S(2)}, u32[]{:S(2)}) collective-permute-start(bf16[2,2,16,1024]{3,2,1,0:T(8,128)(2,1)S(1)} %collective-permute-done.14.refs_1_), channel_id=1, source_target_pairs={{0,32},{4,228},{8,40},{12,236},{16,48},{20,244},{24,56},{28,252},{... | collective-permute-start | bytes 393224 | tf_op jit(solution)/shard_map/ppermute | solution.py:40
  40.7 2.4 %collective-permute-done.15.refs_2_ = bf16[2,2,16,1024]{3,2,1,0:T(8,128)(2,1)S(1)} collective-permute-done((bf16[2,2,16,1024]{3,2,1,0:T(8,128)(2,1)S(1)}, bf16[2,2,16,1024]{3,2,1,0:T(8,128)(2,1)S(1)}, u32[]{:S(2)}, u32[]{:S(2)}) %collective-permute-start.15) | collective-permute-done | bytes 131104 | tf_op jit(solution)/shard_map/ppermute | solution.py:40
  43.0 0.0 collective-permute-start.16
  43.0 0.0 collective-permute-done.8.refs_0_
  43.0 1.5 %collective-permute-start.9 = (bf16[8,1,16,1024]{3,2,1,0:T(8,128)(2,1)S(1)}, bf16[8,1,16,1024]{3,2,1,0:T(8,128)(2,1)S(1)}, u32[]{:S(2)}, u32[]{:S(2)}) collective-permute-start(bf16[8,1,16,1024]{3,2,1,0:T(8,128)(2,1)S(1)} %collective-permute-done.8.refs_0_), channel_id=1, source_target_pairs={{0,224},{4,36},{8,232},{12,44},{16,240},{20,52},{24,248},{28,60},{... | collective-permute-start | bytes 786440 | tf_op jit(solution)/shard_map/ppermute | solution.py:40
  44.5 2.3 %collective-permute-done.16.refs_3_ = bf16[2,2,16,1024]{3,2,1,0:T(8,128)(2,1)S(1)} collective-permute-done((bf16[2,2,16,1024]{3,2,1,0:T(8,128)(2,1)S(1)}, bf16[2,2,16,1024]{3,2,1,0:T(8,128)(2,1)S(1)}, u32[]{:S(2)}, u32[]{:S(2)}) %collective-permute-start.16) | collective-permute-done | bytes 131104 | tf_op jit(solution)/shard_map/ppermute | solution.py:40
  46.8 0.0 collective-permute-done.7.refs_1_
  46.9 0.0 copy-start.2
  46.9 1.6 %collective-permute-start.17 = (bf16[8,2,16,1024]{3,2,1,0:T(8,128)(2,1)S(1)}, bf16[8,2,16,1024]{3,2,1,0:T(8,128)(2,1)S(1)}, u32[]{:S(2)}, u32[]{:S(2)}) collective-permute-start(bf16[8,2,16,1024]{3,2,1,0:T(8,128)(2,1)S(1)} %pack.15.refs_0_), channel_id=1, source_target_pairs={{0,8},{4,28},{8,0},{12,20},{16,24},{20,12},{24,16},{28,4},{32,40},... | collective-permute-start | bytes 1572872 | tf_op jit(solution)/shard_map/ppermute | solution.py:40
  48.5 1.4 %collective-permute-done.9.refs_1_ = bf16[8,1,16,1024]{3,2,1,0:T(8,128)(2,1)S(1)} collective-permute-done((bf16[8,1,16,1024]{3,2,1,0:T(8,128)(2,1)S(1)}, bf16[8,1,16,1024]{3,2,1,0:T(8,128)(2,1)S(1)}, u32[]{:S(2)}, u32[]{:S(2)}) %collective-permute-start.9) | collective-permute-done | bytes 262176 | tf_op jit(solution)/shard_map/ppermute | solution.py:40
  50.0 6.4 %collective-permute-start.10 = (bf16[16,1,16,1024]{3,2,1,0:T(8,128)(2,1)S(1)}, bf16[16,1,16,1024]{3,2,1,0:T(8,128)(2,1)S(1)}, u32[]{:S(2)}, u32[]{:S(2)}) collective-permute-start(bf16[16,1,16,1024]{3,2,1,0:T(8,128)(2,1)S(1)} %pack.13.refs_2_), channel_id=1, source_target_pairs={{0,4},{4,0},{8,12},{12,8},{16,20},{20,16},{24,28},{28,24},{32,36},... | collective-permute-start | bytes 1572872 | tf_op jit(solution)/shard_map/ppermute | solution.py:44
  56.3 0.0 collective-permute-done.17.refs_1_
  56.4 0.5 collective-permute-start.18
  56.9 7.3 %collective-permute-start = (bf16[32,1024]{1,0:T(8,128)(2,1)S(1)}, bf16[32,1024]{1,0:T(8,128)(2,1)S(1)}, u32[]{:S(2)}, u32[]{:S(2)}) collective-permute-start(bf16[32,1024]{1,0:T(8,128)(2,1)S(1)} %copy-done.6), channel_id=1, source_target_pairs={{0,4},{4,0},{8,12},{12,8},{16,20},{20,16},{24,28},{28,24},{32,36},... | collective-permute-start | bytes 196616 | tf_op jit(solution)/shard_map/ppermute | solution.py:281
  64.2 1.9 %collective-permute-start.1 = (bf16[32,1024]{1,0:T(8,128)(2,1)S(1)}, bf16[32,1024]{1,0:T(8,128)(2,1)S(1)}, u32[]{:S(2)}, u32[]{:S(2)}) collective-permute-start(bf16[32,1024]{1,0:T(8,128)(2,1)S(1)} %copy-done.5), channel_id=1, source_target_pairs={{4,8},{12,16},{20,24},{28,32},{36,40},{44,48},{52,56},{60,64},{68,... | collective-permute-start | bytes 196616 | tf_op jit(solution)/shard_map/ppermute | solution.py:283
  66.1 0.0 collective-permute-done.within
  66.1 3.9 %collective-permute-done.1.across = bf16[32,1024]{1,0:T(8,128)(2,1)S(1)} collective-permute-done((bf16[32,1024]{1,0:T(8,128)(2,1)S(1)}, bf16[32,1024]{1,0:T(8,128)(2,1)S(1)}, u32[]{:S(2)}, u32[]{:S(2)}) %collective-permute-start.1) | collective-permute-done | bytes 65568 | tf_op jit(solution)/shard_map/ppermute | solution.py:283
  70.0 0.9 first.1
  71.0 1.3 %collective-permute-start.11 = (f32[16,128]{1,0:T(8,128)S(1)}, f32[16,128]{1,0:T(8,128)S(1)}, u32[]{:S(2)}, u32[]{:S(2)}) collective-permute-start(f32[16,128]{1,0:T(8,128)S(1)} %get-tuple-element.23.a), channel_id=1, source_target_pairs={{0,1},{1,0},{2,3},{3,2},{4,5},{5,4},{6,7},{7,6},{8,9},{9,8},{10,11... | collective-permute-start | bytes 24584 | tf_op jit(solution)/shard_map/ppermute | solution.py:296
  72.3 1.3 %collective-permute-done.11.b = f32[16,128]{1,0:T(8,128)S(1)} collective-permute-done((f32[16,128]{1,0:T(8,128)S(1)}, f32[16,128]{1,0:T(8,128)S(1)}, u32[]{:S(2)}, u32[]{:S(2)}) %collective-permute-start.11) | collective-permute-done | bytes 8224 | tf_op jit(solution)/shard_map/ppermute | solution.py:296
  73.5 2.5 %collective-permute-start.12 = (f32[16,128]{1,0:T(8,128)S(1)}, f32[16,128]{1,0:T(8,128)S(1)}, u32[]{:S(2)}, u32[]{:S(2)}) collective-permute-start(f32[16,128]{1,0:T(8,128)S(1)} %add.1.refs_3_), channel_id=1, source_target_pairs={{0,3},{1,2},{2,1},{3,0},{4,7},{5,6},{6,5},{7,4},{8,11},{9,10},{10,... | collective-permute-start | bytes 24584 | tf_op jit(solution)/shard_map/ppermute | solution.py:303
  76.0 0.0 collective-permute-done.10.refs_3_
  76.0 2.7 %shard_map.46.refs_1_ = f32[1088,1024]{1,0:T(8,128)S(1)} custom-call(bf16[1088,1024]{1,0:T(8,128)(2,1)S(1)} %get-tuple-element.21.x_ref.refs_0_, bf16[3,1024]{1,0:T(4,128)(2,1)S(1)} %copy-done.2, bf16[16,1,16,1024]{3,2,1,0:T(8,128)(2,1)S(1)} %pack.12.refs_0_, bf16[16,1,16,1024]{3,2,1,0:T(8,128)(2,1)S(1)} %collective-permute-done.7.refs_1_, ...), custom_call_target="tpu_custom_call" | custom-call | flops 2281701376 | bytes 6684672 | tf_op jit(solution)/shard_map/pallas_call | solution.py:309
  78.7 0.0 collective-permute-done.12.refs_4_
  78.8 2.1 %shard_map.47 = (bf16[1088,1024]{1,0:T(8,128)(2,1)S(1)}, f32[16,128]{1,0:T(8,128)S(1)}) custom-call(bf16[1088,1024]{1,0:T(8,128)(2,1)S(1)} %get-tuple-element.21.x_ref.refs_0_, f32[1088,1024]{1,0:T(8,128)S(1)} %shard_map.46.refs_1_, bf16[3,1024]{1,0:T(4,128)(2,1)S(1)} %copy-done.3, f32[16,128]{1,0:T(8,128)S(1)} %add.1.refs_3_, ...), custom_call_target="tpu_custom_call" | custom-call | flops 570425344 | bytes 8912896 | tf_op jit(solution)/shard_map/pallas_call | solution.py:325
  80.9 0.0 collective-permute-done.18.refs_1_
  80.9 0.1 pack.17.refs_0_
  81.0 0.1 collective-permute-start.19
  81.1 2.0 %collective-permute-start.23 = (bf16[16,1,16,1024]{3,2,1,0:T(8,128)(2,1)S(1)}, bf16[16,1,16,1024]{3,2,1,0:T(8,128)(2,1)S(1)}, u32[]{:S(2)}, u32[]{:S(2)}) collective-permute-start(bf16[16,1,16,1024]{3,2,1,0:T(8,128)(2,1)S(1)} %pack.18.refs_0_), channel_id=1, source_target_pairs={{0,24},{4,12},{8,16},{12,4},{16,8},{20,28},{24,0},{28,20},{32,56},... | collective-permute-start | bytes 1572872 | tf_op jit(solution)/shard_map/ppermute | solution.py:40
  83.1 0.0 collective-permute-start.20
  83.1 1.2 %collective-permute-start.21 = (f32[16,128]{1,0:T(8,128)S(1)}, f32[16,128]{1,0:T(8,128)S(1)}, u32[]{:S(2)}, u32[]{:S(2)}) collective-permute-start(f32[16,128]{1,0:T(8,128)S(1)} %get-tuple-element.28.refs_3_), channel_id=1, source_target_pairs={{0,3},{1,2},{2,1},{3,0},{4,7},{5,6},{6,5},{7,4},{8,11},{9,10},{10,... | collective-permute-start | bytes 24584 | tf_op jit(solution)/shard_map/ppermute | solution.py:261
  84.3 2.1 %collective-permute-start.22 = (f32[16,128]{1,0:T(8,128)S(1)}, f32[16,128]{1,0:T(8,128)S(1)}, u32[]{:S(2)}, u32[]{:S(2)}) collective-permute-start(f32[16,128]{1,0:T(8,128)S(1)} %get-tuple-element.28.refs_3_), channel_id=1, source_target_pairs={{0,2},{1,3},{2,0},{3,1},{4,6},{5,7},{6,4},{7,5},{8,10},{9,11},{10,... | collective-permute-start | bytes 24584 | tf_op jit(solution)/shard_map/ppermute | solution.py:261
  86.3 0.0 collective-permute-done.19.refs_1_
  86.4 2.7 %shard_map.48.refs_1_ = f32[1088,1024]{1,0:T(8,128)S(1)} custom-call(bf16[1088,1024]{1,0:T(8,128)(2,1)S(1)} %get-tuple-element.25.x_ref.refs_0_, bf16[3,1024]{1,0:T(4,128)(2,1)S(1)} %copy-done.2, bf16[32,1,16,1024]{3,2,1,0:T(8,128)(2,1)S(1)} %pack.17.refs_0_, bf16[32,1,16,1024]{3,2,1,0:T(8,128)(2,1)S(1)} %collective-permute-done.19.refs_1_), custom_call_target="tpu_custom_call" | custom-call | flops 2281701376 | bytes 6684672 | tf_op jit(solution)/shard_map/pallas_call | solution.py:309
  89.1 0.0 collective-permute-done.20.refs_4_
  89.1 2.1 %shard_map.49 = (bf16[1088,1024]{1,0:T(8,128)(2,1)S(1)}, f32[16,128]{1,0:T(8,128)S(1)}) custom-call(bf16[1088,1024]{1,0:T(8,128)(2,1)S(1)} %get-tuple-element.25.x_ref.refs_0_, f32[1088,1024]{1,0:T(8,128)S(1)} %shard_map.48.refs_1_, bf16[3,1024]{1,0:T(4,128)(2,1)S(1)} %copy-done.3, f32[16,128]{1,0:T(8,128)S(1)} %get-tuple-element.28.refs_3_, ...), custom_call_target="tpu_custom_call" | custom-call | flops 570425344 | bytes 8912896 | tf_op jit(solution)/shard_map/pallas_call | solution.py:325
  91.2 0.1 pack.19.refs_0_
  91.3 2.9 %collective-permute-start.24 = (bf16[32,1,16,1024]{3,2,1,0:T(8,128)(2,1)S(1)}, bf16[32,1,16,1024]{3,2,1,0:T(8,128)(2,1)S(1)}, u32[]{:S(2)}, u32[]{:S(2)}) collective-permute-start(bf16[32,1,16,1024]{3,2,1,0:T(8,128)(2,1)S(1)} %pack.19.refs_0_), channel_id=1, source_target_pairs={{0,4},{4,0},{8,12},{12,8},{16,20},{20,16},{24,28},{28,24},{32,36},... | collective-permute-start | bytes 3145736 | tf_op jit(solution)/shard_map/ppermute | solution.py:44
  94.1 0.7 collective-permute-start.25
  94.9 1.7 %collective-permute-start.26 = (f32[16,128]{1,0:T(8,128)S(1)}, f32[16,128]{1,0:T(8,128)S(1)}, u32[]{:S(2)}, u32[]{:S(2)}) collective-permute-start(f32[16,128]{1,0:T(8,128)S(1)} %get-tuple-element.31.refs_3_), channel_id=1, source_target_pairs={{0,3},{1,2},{2,1},{3,0},{4,7},{5,6},{6,5},{7,4},{8,11},{9,10},{10,... | collective-permute-start | bytes 24584 | tf_op jit(solution)/shard_map/ppermute | solution.py:261
  96.6 0.8 collective-permute-start.27
  97.4 2.7 %shard_map.50.refs_1_ = f32[1088,1024]{1,0:T(8,128)S(1)} custom-call(bf16[1088,1024]{1,0:T(8,128)(2,1)S(1)} %get-tuple-element.30.x_ref.refs_0_, bf16[3,1024]{1,0:T(4,128)(2,1)S(1)} %copy-done.2, bf16[32,1,16,1024]{3,2,1,0:T(8,128)(2,1)S(1)} %pack.19.refs_0_, bf16[32,1,16,1024]{3,2,1,0:T(8,128)(2,1)S(1)} %collective-permute-done.24.refs_1_), custom_call_target="tpu_custom_call" | custom-call | flops 2281701376 | bytes 6684672 | tf_op jit(solution)/shard_map/pallas_call | solution.py:309
  100.1 0.0 collective-permute-done.25.refs_4_
  100.1 0.5 collective-permute-done.27.refs_6_
  100.6 2.3 %shard_map.51 = bf16[1024,1024]{1,0:T(8,128)(2,1)} custom-call(bf16[1088,1024]{1,0:T(8,128)(2,1)S(1)} %get-tuple-element.30.x_ref.refs_0_, f32[1088,1024]{1,0:T(8,128)S(1)} %shard_map.50.refs_1_, bf16[3,1024]{1,0:T(4,128)(2,1)S(1)} %copy-done.3, f32[16,128]{1,0:T(8,128)S(1)} %get-tuple-element.31.refs_3_, f32[16,128]{1,0:T(8,128)S(1)} %collective-permute-done.25.refs_4_, ...), custom_call_target="tpu_custom_call" | custom-call | flops 570425344 | bytes 8912896 | tf_op jit(solution)/shard_map/pallas_call | solution.py:325
  (25 shorter events, 0.2 us)
Async XLA Ops:
  0.0 28.0 %copy-start.4 = (bf16[3,1,16,1024]{3,2,1,0:T(8,128)(2,1)S(1)}, bf16[3,1,16,1024]{3,2,1,0:T(8,128)(2,1)}, u32[]{:S(2)}) copy-start(bf16[3,1,16,1024]{3,2,1,0:T(8,128)(2,1)} %param.6) | copy-start | bytes 294916
  0.0 6.5 %collective-permute-start.2 = (bf16[1,3,16,1024]{3,2,1,0:T(8,128)(2,1)}, bf16[1,3,16,1024]{3,2,1,0:T(8,128)(2,1)S(1)}, u32[]{:S(2)}, u32[]{:S(2)}) collective-permute-start(bf16[1,3,16,1024]{3,2,1,0:T(8,128)(2,1)} %bitcast.1), channel_id=1, source_target_pairs={{0,8},{4,28},{8,0},{12,20},{16,24},{20,12},{24,16},{28,4},{32,40},... | collective-permute-start | bytes 294920 | tf_op jit(solution)/shard_map/ppermute | solution.py:40
  3.6 4.9 %collective-permute-start.3 = (bf16[1,3,16,1024]{3,2,1,0:T(8,128)(2,1)}, bf16[1,3,16,1024]{3,2,1,0:T(8,128)(2,1)S(1)}, u32[]{:S(2)}, u32[]{:S(2)}) collective-permute-start(bf16[1,3,16,1024]{3,2,1,0:T(8,128)(2,1)} %bitcast.2), channel_id=1, source_target_pairs={{0,24},{4,12},{8,16},{12,4},{16,8},{20,28},{24,0},{28,20},{32,56},... | collective-permute-start | bytes 294920 | tf_op jit(solution)/shard_map/ppermute | solution.py:40
  3.6 5.7 %collective-permute-start.4 = (bf16[1,3,16,1024]{3,2,1,0:T(8,128)(2,1)}, bf16[1,3,16,1024]{3,2,1,0:T(8,128)(2,1)S(1)}, u32[]{:S(2)}, u32[]{:S(2)}) collective-permute-start(bf16[1,3,16,1024]{3,2,1,0:T(8,128)(2,1)} %bitcast.3), channel_id=1, source_target_pairs={{0,16},{4,20},{8,24},{12,28},{16,0},{20,4},{24,8},{28,12},{32,48},... | collective-permute-start | bytes 294920 | tf_op jit(solution)/shard_map/ppermute | solution.py:40
  9.2 0.9 copy-start.1
  10.1 8.0 %collective-permute-start.5 = (bf16[4,1,16,1024]{3,2,1,0:T(8,128)(2,1)S(1)}, bf16[4,1,16,1024]{3,2,1,0:T(8,128)(2,1)S(1)}, u32[]{:S(2)}, u32[]{:S(2)}) collective-permute-start(bf16[4,1,16,1024]{3,2,1,0:T(8,128)(2,1)S(1)} %pack.10.refs_0_), channel_id=1, source_target_pairs={{0,32},{4,228},{8,40},{12,236},{16,48},{20,244},{24,56},{28,252},{... | collective-permute-start | bytes 393224 | tf_op jit(solution)/shard_map/ppermute | solution.py:40
  18.2 5.3 %collective-permute-start.6 = (bf16[8,1,16,1024]{3,2,1,0:T(8,128)(2,1)S(1)}, bf16[8,1,16,1024]{3,2,1,0:T(8,128)(2,1)S(1)}, u32[]{:S(2)}, u32[]{:S(2)}) collective-permute-start(bf16[8,1,16,1024]{3,2,1,0:T(8,128)(2,1)S(1)} %pack.11.refs_0_), channel_id=1, source_target_pairs={{0,224},{4,36},{8,232},{12,44},{16,240},{20,52},{24,248},{28,60},{... | collective-permute-start | bytes 786440 | tf_op jit(solution)/shard_map/ppermute | solution.py:40
  23.5 33.3 %copy-start.6 = (bf16[32,1024]{1,0:T(8,128)(2,1)S(1)}, bf16[32,1024]{1,0:T(8,128)(2,1)}, u32[]{:S(2)}) copy-start(bf16[32,1024]{1,0:T(8,128)(2,1)} %get-tuple-element.19) | copy-start | bytes 196612
  23.6 40.6 %copy-start.5 = (bf16[32,1024]{1,0:T(8,128)(2,1)S(1)}, bf16[32,1024]{1,0:T(8,128)(2,1)}, u32[]{:S(2)}) copy-start(bf16[32,1024]{1,0:T(8,128)(2,1)} %get-tuple-element.20) | copy-start | bytes 196612
  23.6 46.5 %copy-start = (bf16[1024,1024]{1,0:T(8,128)(2,1)S(1)}, bf16[1024,1024]{1,0:T(8,128)(2,1)}, u32[]{:S(2)}) copy-start(bf16[1024,1024]{1,0:T(8,128)(2,1)} %x.3) | copy-start | bytes 6291460
  23.6 23.3 %collective-permute-start.7 = (bf16[16,1,16,1024]{3,2,1,0:T(8,128)(2,1)S(1)}, bf16[16,1,16,1024]{3,2,1,0:T(8,128)(2,1)S(1)}, u32[]{:S(2)}, u32[]{:S(2)}) collective-permute-start(bf16[16,1,16,1024]{3,2,1,0:T(8,128)(2,1)S(1)} %pack.12.refs_0_), channel_id=1, source_target_pairs={{0,4},{4,0},{8,12},{12,8},{16,20},{20,16},{24,28},{28,24},{32,36},... | collective-permute-start | bytes 1572872 | tf_op jit(solution)/shard_map/ppermute | solution.py:44
  28.0 5.0 %collective-permute-start.13 = (bf16[1,3,16,1024]{3,2,1,0:T(8,128)(2,1)S(1)}, bf16[1,3,16,1024]{3,2,1,0:T(8,128)(2,1)S(1)}, u32[]{:S(2)}, u32[]{:S(2)}) collective-permute-start(bf16[1,3,16,1024]{3,2,1,0:T(8,128)(2,1)S(1)} %bitcast.5), channel_id=1, source_target_pairs={{0,32},{4,228},{8,40},{12,236},{16,48},{20,244},{24,56},{28,252},{... | collective-permute-start | bytes 294920 | tf_op jit(solution)/shard_map/ppermute | solution.py:40
  33.0 3.9 %collective-permute-start.14 = (bf16[2,2,16,1024]{3,2,1,0:T(8,128)(2,1)S(1)}, bf16[2,2,16,1024]{3,2,1,0:T(8,128)(2,1)S(1)}, u32[]{:S(2)}, u32[]{:S(2)}) collective-permute-start(bf16[2,2,16,1024]{3,2,1,0:T(8,128)(2,1)S(1)} %pack.14.refs_0_), channel_id=1, source_target_pairs={{0,224},{4,36},{8,232},{12,44},{16,240},{20,52},{24,248},{28,60},{... | collective-permute-start | bytes 393224 | tf_op jit(solution)/shard_map/ppermute | solution.py:40
  33.1 9.9 %collective-permute-start.8 = (bf16[8,1,16,1024]{3,2,1,0:T(8,128)(2,1)S(1)}, bf16[8,1,16,1024]{3,2,1,0:T(8,128)(2,1)S(1)}, u32[]{:S(2)}, u32[]{:S(2)}) collective-permute-start(bf16[8,1,16,1024]{3,2,1,0:T(8,128)(2,1)S(1)} %collective-permute-done.6.refs_1_), channel_id=1, source_target_pairs={{0,32},{4,228},{8,40},{12,236},{16,48},{20,244},{24,56},{28,252},{... | collective-permute-start | bytes 786440 | tf_op jit(solution)/shard_map/ppermute | solution.py:40
  36.9 6.1 %collective-permute-start.15 = (bf16[2,2,16,1024]{3,2,1,0:T(8,128)(2,1)S(1)}, bf16[2,2,16,1024]{3,2,1,0:T(8,128)(2,1)S(1)}, u32[]{:S(2)}, u32[]{:S(2)}) collective-permute-start(bf16[2,2,16,1024]{3,2,1,0:T(8,128)(2,1)S(1)} %collective-permute-done.14.refs_1_), channel_id=1, source_target_pairs={{0,32},{4,228},{8,40},{12,236},{16,48},{20,244},{24,56},{28,252},{... | collective-permute-start | bytes 393224 | tf_op jit(solution)/shard_map/ppermute | solution.py:40
  43.0 3.8 %collective-permute-start.16 = (bf16[2,2,16,1024]{3,2,1,0:T(8,128)(2,1)S(1)}, bf16[2,2,16,1024]{3,2,1,0:T(8,128)(2,1)S(1)}, u32[]{:S(2)}, u32[]{:S(2)}) collective-permute-start(bf16[2,2,16,1024]{3,2,1,0:T(8,128)(2,1)S(1)} %collective-permute-done.15.refs_2_), channel_id=1, source_target_pairs={{0,224},{4,36},{8,232},{12,44},{16,240},{20,52},{24,248},{28,60},{... | collective-permute-start | bytes 393224 | tf_op jit(solution)/shard_map/ppermute | solution.py:40
  43.0 6.9 %collective-permute-start.9 = (bf16[8,1,16,1024]{3,2,1,0:T(8,128)(2,1)S(1)}, bf16[8,1,16,1024]{3,2,1,0:T(8,128)(2,1)S(1)}, u32[]{:S(2)}, u32[]{:S(2)}) collective-permute-start(bf16[8,1,16,1024]{3,2,1,0:T(8,128)(2,1)S(1)} %collective-permute-done.8.refs_0_), channel_id=1, source_target_pairs={{0,224},{4,36},{8,232},{12,44},{16,240},{20,52},{24,248},{28,60},{... | collective-permute-start | bytes 786440 | tf_op jit(solution)/shard_map/ppermute | solution.py:40
  46.9 29.2 %copy-start.2 = (bf16[3,1024]{1,0:T(4,128)(2,1)S(1)}, bf16[3,1024]{1,0:T(4,128)(2,1)}, u32[]{:S(2)}) copy-start(bf16[3,1024]{1,0:T(4,128)(2,1)} %gain_ref.5) | copy-start | bytes 18436
  46.9 9.4 %collective-permute-start.17 = (bf16[8,2,16,1024]{3,2,1,0:T(8,128)(2,1)S(1)}, bf16[8,2,16,1024]{3,2,1,0:T(8,128)(2,1)S(1)}, u32[]{:S(2)}, u32[]{:S(2)}) collective-permute-start(bf16[8,2,16,1024]{3,2,1,0:T(8,128)(2,1)S(1)} %pack.15.refs_0_), channel_id=1, source_target_pairs={{0,8},{4,28},{8,0},{12,20},{16,24},{20,12},{24,16},{28,4},{32,40},... | collective-permute-start | bytes 1572872 | tf_op jit(solution)/shard_map/ppermute | solution.py:40
  50.0 26.0 %collective-permute-start.10 = (bf16[16,1,16,1024]{3,2,1,0:T(8,128)(2,1)S(1)}, bf16[16,1,16,1024]{3,2,1,0:T(8,128)(2,1)S(1)}, u32[]{:S(2)}, u32[]{:S(2)}) collective-permute-start(bf16[16,1,16,1024]{3,2,1,0:T(8,128)(2,1)S(1)} %pack.13.refs_2_), channel_id=1, source_target_pairs={{0,4},{4,0},{8,12},{12,8},{16,20},{20,16},{24,28},{28,24},{32,36},... | collective-permute-start | bytes 1572872 | tf_op jit(solution)/shard_map/ppermute | solution.py:44
  56.4 24.5 %collective-permute-start.18 = (bf16[16,1,16,1024]{3,2,1,0:T(8,128)(2,1)S(1)}, bf16[16,1,16,1024]{3,2,1,0:T(8,128)(2,1)S(1)}, u32[]{:S(2)}, u32[]{:S(2)}) collective-permute-start(bf16[16,1,16,1024]{3,2,1,0:T(8,128)(2,1)S(1)} %pack.16.refs_0_), channel_id=1, source_target_pairs={{0,24},{4,12},{8,16},{12,4},{16,8},{20,28},{24,0},{28,20},{32,56},... | collective-permute-start | bytes 1572872 | tf_op jit(solution)/shard_map/ppermute | solution.py:40
  56.9 9.2 %collective-permute-start = (bf16[32,1024]{1,0:T(8,128)(2,1)S(1)}, bf16[32,1024]{1,0:T(8,128)(2,1)S(1)}, u32[]{:S(2)}, u32[]{:S(2)}) collective-permute-start(bf16[32,1024]{1,0:T(8,128)(2,1)S(1)} %copy-done.6), channel_id=1, source_target_pairs={{0,4},{4,0},{8,12},{12,8},{16,20},{20,16},{24,28},{28,24},{32,36},... | collective-permute-start | bytes 196616 | tf_op jit(solution)/shard_map/ppermute | solution.py:281
  64.2 5.9 %collective-permute-start.1 = (bf16[32,1024]{1,0:T(8,128)(2,1)S(1)}, bf16[32,1024]{1,0:T(8,128)(2,1)S(1)}, u32[]{:S(2)}, u32[]{:S(2)}) collective-permute-start(bf16[32,1024]{1,0:T(8,128)(2,1)S(1)} %copy-done.5), channel_id=1, source_target_pairs={{4,8},{12,16},{20,24},{28,32},{36,40},{44,48},{52,56},{60,64},{68,... | collective-permute-start | bytes 196616 | tf_op jit(solution)/shard_map/ppermute | solution.py:283
  71.0 2.6 %collective-permute-start.11 = (f32[16,128]{1,0:T(8,128)S(1)}, f32[16,128]{1,0:T(8,128)S(1)}, u32[]{:S(2)}, u32[]{:S(2)}) collective-permute-start(f32[16,128]{1,0:T(8,128)S(1)} %get-tuple-element.23.a), channel_id=1, source_target_pairs={{0,1},{1,0},{2,3},{3,2},{4,5},{5,4},{6,7},{7,6},{8,9},{9,8},{10,11... | collective-permute-start | bytes 24584 | tf_op jit(solution)/shard_map/ppermute | solution.py:296
  73.5 5.2 %collective-permute-start.12 = (f32[16,128]{1,0:T(8,128)S(1)}, f32[16,128]{1,0:T(8,128)S(1)}, u32[]{:S(2)}, u32[]{:S(2)}) collective-permute-start(f32[16,128]{1,0:T(8,128)S(1)} %add.1.refs_3_), channel_id=1, source_target_pairs={{0,3},{1,2},{2,1},{3,0},{4,7},{5,6},{6,5},{7,4},{8,11},{9,10},{10,... | collective-permute-start | bytes 24584 | tf_op jit(solution)/shard_map/ppermute | solution.py:303
  76.0 2.7 %copy-start.3 = (bf16[3,1024]{1,0:T(4,128)(2,1)S(1)}, bf16[3,1024]{1,0:T(4,128)(2,1)}, u32[]{:S(2)}) copy-start(bf16[3,1024]{1,0:T(4,128)(2,1)} %refs_2_.5) | copy-start | bytes 18436
  81.0 5.4 %collective-permute-start.19 = (bf16[32,1,16,1024]{3,2,1,0:T(8,128)(2,1)S(1)}, bf16[32,1,16,1024]{3,2,1,0:T(8,128)(2,1)S(1)}, u32[]{:S(2)}, u32[]{:S(2)}) collective-permute-start(bf16[32,1,16,1024]{3,2,1,0:T(8,128)(2,1)S(1)} %pack.17.refs_0_), channel_id=1, source_target_pairs={{0,4},{4,0},{8,12},{12,8},{16,20},{20,16},{24,28},{28,24},{32,36},... | collective-permute-start | bytes 3145736 | tf_op jit(solution)/shard_map/ppermute | solution.py:44
  81.1 10.1 %collective-permute-start.23 = (bf16[16,1,16,1024]{3,2,1,0:T(8,128)(2,1)S(1)}, bf16[16,1,16,1024]{3,2,1,0:T(8,128)(2,1)S(1)}, u32[]{:S(2)}, u32[]{:S(2)}) collective-permute-start(bf16[16,1,16,1024]{3,2,1,0:T(8,128)(2,1)S(1)} %pack.18.refs_0_), channel_id=1, source_target_pairs={{0,24},{4,12},{8,16},{12,4},{16,8},{20,28},{24,0},{28,20},{32,56},... | collective-permute-start | bytes 1572872 | tf_op jit(solution)/shard_map/ppermute | solution.py:40
  83.1 6.0 %collective-permute-start.20 = (f32[16,128]{1,0:T(8,128)S(1)}, f32[16,128]{1,0:T(8,128)S(1)}, u32[]{:S(2)}, u32[]{:S(2)}) collective-permute-start(f32[16,128]{1,0:T(8,128)S(1)} %get-tuple-element.28.refs_3_), channel_id=1, source_target_pairs={{0,1},{1,0},{2,3},{3,2},{4,5},{5,4},{6,7},{7,6},{8,9},{9,8},{10,11... | collective-permute-start | bytes 24584 | tf_op jit(solution)/shard_map/ppermute | solution.py:261
  83.1 6.0 %collective-permute-start.21 = (f32[16,128]{1,0:T(8,128)S(1)}, f32[16,128]{1,0:T(8,128)S(1)}, u32[]{:S(2)}, u32[]{:S(2)}) collective-permute-start(f32[16,128]{1,0:T(8,128)S(1)} %get-tuple-element.28.refs_3_), channel_id=1, source_target_pairs={{0,3},{1,2},{2,1},{3,0},{4,7},{5,6},{6,5},{7,4},{8,11},{9,10},{10,... | collective-permute-start | bytes 24584 | tf_op jit(solution)/shard_map/ppermute | solution.py:261
  84.3 4.8 %collective-permute-start.22 = (f32[16,128]{1,0:T(8,128)S(1)}, f32[16,128]{1,0:T(8,128)S(1)}, u32[]{:S(2)}, u32[]{:S(2)}) collective-permute-start(f32[16,128]{1,0:T(8,128)S(1)} %get-tuple-element.28.refs_3_), channel_id=1, source_target_pairs={{0,2},{1,3},{2,0},{3,1},{4,6},{5,7},{6,4},{7,5},{8,10},{9,11},{10,... | collective-permute-start | bytes 24584 | tf_op jit(solution)/shard_map/ppermute | solution.py:261
  91.3 6.1 %collective-permute-start.24 = (bf16[32,1,16,1024]{3,2,1,0:T(8,128)(2,1)S(1)}, bf16[32,1,16,1024]{3,2,1,0:T(8,128)(2,1)S(1)}, u32[]{:S(2)}, u32[]{:S(2)}) collective-permute-start(bf16[32,1,16,1024]{3,2,1,0:T(8,128)(2,1)S(1)} %pack.19.refs_0_), channel_id=1, source_target_pairs={{0,4},{4,0},{8,12},{12,8},{16,20},{20,16},{24,28},{28,24},{32,36},... | collective-permute-start | bytes 3145736 | tf_op jit(solution)/shard_map/ppermute | solution.py:44
  94.1 5.9 %collective-permute-start.25 = (f32[16,128]{1,0:T(8,128)S(1)}, f32[16,128]{1,0:T(8,128)S(1)}, u32[]{:S(2)}, u32[]{:S(2)}) collective-permute-start(f32[16,128]{1,0:T(8,128)S(1)} %get-tuple-element.31.refs_3_), channel_id=1, source_target_pairs={{0,1},{1,0},{2,3},{3,2},{4,5},{5,4},{6,7},{7,6},{8,9},{9,8},{10,11... | collective-permute-start | bytes 24584 | tf_op jit(solution)/shard_map/ppermute | solution.py:261
  94.9 5.2 %collective-permute-start.26 = (f32[16,128]{1,0:T(8,128)S(1)}, f32[16,128]{1,0:T(8,128)S(1)}, u32[]{:S(2)}, u32[]{:S(2)}) collective-permute-start(f32[16,128]{1,0:T(8,128)S(1)} %get-tuple-element.31.refs_3_), channel_id=1, source_target_pairs={{0,3},{1,2},{2,1},{3,0},{4,7},{5,6},{6,5},{7,4},{8,11},{9,10},{10,... | collective-permute-start | bytes 24584 | tf_op jit(solution)/shard_map/ppermute | solution.py:261
  96.6 4.0 %collective-permute-start.27 = (f32[16,128]{1,0:T(8,128)S(1)}, f32[16,128]{1,0:T(8,128)S(1)}, u32[]{:S(2)}, u32[]{:S(2)}) collective-permute-start(f32[16,128]{1,0:T(8,128)S(1)} %get-tuple-element.31.refs_3_), channel_id=1, source_target_pairs={{0,2},{1,3},{2,0},{3,1},{4,6},{5,7},{6,4},{7,5},{8,10},{9,11},{10,... | collective-permute-start | bytes 24584 | tf_op jit(solution)/shard_map/ppermute | solution.py:261
where the time goes:
time: 103 us
  starting transfers between devices  59 us (57%)
  waiting for transfers between devices  25.2 us (24%)
  Pallas kernels  17.6 us (17%)
    ppermute x14, starting transfers between devices, trade(): return lax.ppermute(value, 'sp', found)  25.7 us
    ppermute x14, waiting for transfers between devices, trade(): return lax.ppermute(value, 'sp', found)  19.5 us
    ppermute x4, starting transfers between devices, partner(): return lax.ppermute(value, 'sp', [(sp, sp ^ 1) for sp in range(Z * Y * C)])  13.7 us
    pallas_call x3, Pallas kernels, program(): pl.pallas_call(functools.partial(map_kernel, layer, [p[1:] for p in piece...  8.06 us
    ppermute x1, starting transfers between devices, program(): within = lax.ppermute(within, 'sp', [(i, i ^ 1) for i in range(devices)])  7.31 us
    pallas_call x3, Pallas kernels, program(): pl.pallas_call(functools.partial(pool_kernel, layer, lo, hi, last, rows *...  6.58 us
    ppermute x6, starting transfers between devices, over_tp(): found.append(lax.ppermute(sums, 'tp', [(i, i ^ k) for i in range(n)]))  6.51 us
    ppermute x1, waiting for transfers between devices, program(): across = lax.ppermute(across, 'sp', pairs + [(j, i) for i, j in pairs])  3.94 us
  transfers between devices with their start and end apart: 28, of which 12 were waited for; matrix products, arithmetic and copies ran while one was open for 0% of the time, Pallas kernels for 15%

commit v1 on v0

--- a/solution.py
+++ b/solution.py
@@ -96,8 +96,8 @@
     two = pack((fetched, behind), 1, layers)
     second = trade(two, "z", 2)
     third = trade(second, "z", 1)
-    line = pack((two, second, third, after(trade(third, "z", 2), early)), 0, layers - 1)
-    beside = after(trade(line, "y", 1), fourth)
+    line = pack((two, second, third, trade(third, "z", 2)), 0, layers - 1)
+    beside = trade(line, "y", 1)
     for i in range(layers - 1):
         near = pack((line, beside), i, i + 1)
         far = trade(near, "y", 2)
@@ -186,7 +186,7 @@
             w[pl.ds(pl.multiple_of(at * 16, 16), 16), :] = ref[j, 0]
 
     gain = gain_ref[layer : layer + 1, :].astype(jnp.float32)
-    step = 272
+    step = 1088
     for i in range(0, total, step):
         scaled = (x_ref[i : i + step].astype(jnp.float32) * gain).astype(jnp.bfloat16)
         for j in range(0, width, 256):
@@ -275,7 +275,7 @@
         in_specs=[pl.BlockSpec(memory_space=pltpu.HBM)] * 2,
         out_specs=(VMEM,) * 3,
         scratch_shapes=[pltpu.VMEM((2, HALO, width), stream.dtype), pltpu.SemaphoreType.DMA((3,))],
-        compiler_params=pltpu.CompilerParams(vmem_limit_bytes=125 * 2**19),
+        compiler_params=pltpu.CompilerParams(vmem_limit_bytes=123 * 2**19),
         name="prepare",
     )(own, stream)
     within = lax.ppermute(within, "sp", [(i, i ^ 1) for i in range(devices)])

time: 103 us -> 101 us (0.981)
  waiting for transfers between devices: 25.2 us -> 20.4 us
  starting transfers between devices: 59 us -> 61.7 us
    ppermute x14, waiting for transfers between devices: 19.5 us -> 14.7 us  [trade(): return lax.ppermute(value, 'sp', found)]
    ppermute x1, starting transfers between devices: 7.31 us -> 10.8 us  [program(): within = lax.ppermute(within, 'sp', [(i, i ^ 1) for i in range(devices)])]
  transfers between devices with their start and end apart: 28 -> 28, of which waited for: 12 -> 10; matrix products, arithmetic and copies ran while one was open for 0% -> 0% of each run, Pallas kernels for 15% -> 15%
where the time goes in v1:
time: 101 us
  starting transfers between devices  61.7 us (61%)
  waiting for transfers between devices  20.4 us (20%)
  Pallas kernels  17.6 us (17%)
    ppermute x14, starting transfers between devices, trade(): return lax.ppermute(value, 'sp', found)  25.8 us
    ppermute x14, waiting for transfers between devices, trade(): return lax.ppermute(value, 'sp', found)  14.7 us
    ppermute x4, starting transfers between devices, partner(): return lax.ppermute(value, 'sp', [(sp, sp ^ 1) for sp in range(Z * Y * C)])  12.9 us
    ppermute x1, starting transfers between devices, program(): within = lax.ppermute(within, 'sp', [(i, i ^ 1) for i in range(devices)])  10.8 us
    pallas_call x3, Pallas kernels, program(): pl.pallas_call(functools.partial(map_kernel, layer, [p[1:] for p in piece...  8.05 us
    pallas_call x3, Pallas kernels, program(): pl.pallas_call(functools.partial(pool_kernel, layer, lo, hi, last, rows *...  6.58 us
    ppermute x6, starting transfers between devices, over_tp(): found.append(lax.ppermute(sums, 'tp', [(i, i ^ k) for i in range(n)]))  6.51 us
    ppermute x1, waiting for transfers between devices, program(): across = lax.ppermute(across, 'sp', pairs + [(j, i) for i, j in pairs])  3.94 us
  transfers between devices with their start and end apart: 28, of which 10 were waited for; matrix products, arithmetic and copies ran while one was open for 0% of the time, Pallas kernels for 15%

profile of v1, /device:TPU:1, one launch (start us, length us, event | category | flops | bytes accessed | tf_op | source)
XLA Modules:
  0.0 101.0 jit_solution(1256386827599523307)
XLA Ops:
  0.0 3.6 %collective-permute-start.2 = (bf16[1,3,16,1024]{3,2,1,0:T(8,128)(2,1)}, bf16[1,3,16,1024]{3,2,1,0:T(8,128)(2,1)S(1)}, u32[]{:S(2)}, u32[]{:S(2)}) collective-permute-start(bf16[1,3,16,1024]{3,2,1,0:T(8,128)(2,1)} %bitcast.1), channel_id=1, source_target_pairs={{0,8},{4,28},{8,0},{12,20},{16,24},{20,12},{24,16},{28,4},{32,40},... | collective-permute-start | bytes 294920 | tf_op jit(solution)/shard_map/ppermute | solution.py:40
  3.6 0.0 collective-permute-start.3
  3.6 1.3 %collective-permute-start.4 = (bf16[1,3,16,1024]{3,2,1,0:T(8,128)(2,1)}, bf16[1,3,16,1024]{3,2,1,0:T(8,128)(2,1)S(1)}, u32[]{:S(2)}, u32[]{:S(2)}) collective-permute-start(bf16[1,3,16,1024]{3,2,1,0:T(8,128)(2,1)} %bitcast.3), channel_id=1, source_target_pairs={{0,16},{4,20},{8,24},{12,28},{16,0},{20,4},{24,8},{28,12},{32,48},... | collective-permute-start | bytes 294920 | tf_op jit(solution)/shard_map/ppermute | solution.py:40
  4.8 1.7 %prepare.1 = (bf16[1,3,16,1024]{3,2,1,0:T(8,128)(2,1)}, bf16[32,1024]{1,0:T(8,128)(2,1)}, bf16[32,1024]{1,0:T(8,128)(2,1)}) custom-call(bf16[1,3,16,1024]{3,2,1,0:T(8,128)(2,1)} %bitcast.4, bf16[1024,1024]{1,0:T(8,128)(2,1)} %x.3), custom_call_target="tpu_custom_call" | custom-call | tf_op jit(solution)/shard_map/prepare/pallas_call | solution.py:272
  6.5 0.0 collective-permute-done.2.refs_1_
  6.5 2.0 %collective-permute-done.3.refs_2_ = bf16[1,3,16,1024]{3,2,1,0:T(8,128)(2,1)S(1)} collective-permute-done((bf16[1,3,16,1024]{3,2,1,0:T(8,128)(2,1)}, bf16[1,3,16,1024]{3,2,1,0:T(8,128)(2,1)S(1)}, u32[]{:S(2)}, u32[]{:S(2)}) %collective-permute-start.3) | collective-permute-done | bytes 98336 | tf_op jit(solution)/shard_map/ppermute | solution.py:40
  8.5 0.8 collective-permute-done.4.refs_3_
  9.2 0.9 copy-done.1
  10.1 5.7 %collective-permute-start.5 = (bf16[4,1,16,1024]{3,2,1,0:T(8,128)(2,1)S(1)}, bf16[4,1,16,1024]{3,2,1,0:T(8,128)(2,1)S(1)}, u32[]{:S(2)}, u32[]{:S(2)}) collective-permute-start(bf16[4,1,16,1024]{3,2,1,0:T(8,128)(2,1)S(1)} %pack.10.refs_0_), channel_id=1, source_target_pairs={{0,32},{4,228},{8,40},{12,236},{16,48},{20,244},{24,56},{28,252},{... | collective-permute-start | bytes 393224 | tf_op jit(solution)/shard_map/ppermute | solution.py:40
  15.8 2.4 %collective-permute-done.5.refs_1_ = bf16[4,1,16,1024]{3,2,1,0:T(8,128)(2,1)S(1)} collective-permute-done((bf16[4,1,16,1024]{3,2,1,0:T(8,128)(2,1)S(1)}, bf16[4,1,16,1024]{3,2,1,0:T(8,128)(2,1)S(1)}, u32[]{:S(2)}, u32[]{:S(2)}) %collective-permute-start.5) | collective-permute-done | bytes 131104 | tf_op jit(solution)/shard_map/ppermute | solution.py:40
  18.2 0.1 collective-permute-start.6
  18.3 2.8 %collective-permute-start.13 = (bf16[1,3,16,1024]{3,2,1,0:T(8,128)(2,1)S(1)}, bf16[1,3,16,1024]{3,2,1,0:T(8,128)(2,1)S(1)}, u32[]{:S(2)}, u32[]{:S(2)}) collective-permute-start(bf16[1,3,16,1024]{3,2,1,0:T(8,128)(2,1)S(1)} %bitcast.5), channel_id=1, source_target_pairs={{0,32},{4,228},{8,40},{12,236},{16,48},{20,244},{24,56},{28,252},{... | collective-permute-start | bytes 294920 | tf_op jit(solution)/shard_map/ppermute | solution.py:40
  21.1 2.0 %collective-permute-done.13.refs_1_ = bf16[1,3,16,1024]{3,2,1,0:T(8,128)(2,1)S(1)} collective-permute-done((bf16[1,3,16,1024]{3,2,1,0:T(8,128)(2,1)S(1)}, bf16[1,3,16,1024]{3,2,1,0:T(8,128)(2,1)S(1)}, u32[]{:S(2)}, u32[]{:S(2)}) %collective-permute-start.13) | collective-permute-done | bytes 98336 | tf_op jit(solution)/shard_map/ppermute | solution.py:40
  23.1 0.0 copy-start
  23.1 1.6 %collective-permute-start.14 = (bf16[2,2,16,1024]{3,2,1,0:T(8,128)(2,1)S(1)}, bf16[2,2,16,1024]{3,2,1,0:T(8,128)(2,1)S(1)}, u32[]{:S(2)}, u32[]{:S(2)}) collective-permute-start(bf16[2,2,16,1024]{3,2,1,0:T(8,128)(2,1)S(1)} %pack.14.refs_0_), channel_id=1, source_target_pairs={{0,224},{4,36},{8,232},{12,44},{16,240},{20,52},{24,248},{28,60},{... | collective-permute-start | bytes 393224 | tf_op jit(solution)/shard_map/ppermute | solution.py:40
  24.7 0.0 collective-permute-done.6.refs_1_
  24.7 1.5 %collective-permute-start.8 = (bf16[8,1,16,1024]{3,2,1,0:T(8,128)(2,1)S(1)}, bf16[8,1,16,1024]{3,2,1,0:T(8,128)(2,1)S(1)}, u32[]{:S(2)}, u32[]{:S(2)}) collective-permute-start(bf16[8,1,16,1024]{3,2,1,0:T(8,128)(2,1)S(1)} %collective-permute-done.6.refs_1_), channel_id=1, source_target_pairs={{0,32},{4,228},{8,40},{12,236},{16,48},{20,244},{24,56},{28,252},{... | collective-permute-start | bytes 786440 | tf_op jit(solution)/shard_map/ppermute | solution.py:40
  26.2 1.8 %collective-permute-done.14.refs_1_ = bf16[2,2,16,1024]{3,2,1,0:T(8,128)(2,1)S(1)} collective-permute-done((bf16[2,2,16,1024]{3,2,1,0:T(8,128)(2,1)S(1)}, bf16[2,2,16,1024]{3,2,1,0:T(8,128)(2,1)S(1)}, u32[]{:S(2)}, u32[]{:S(2)}) %collective-permute-start.14) | collective-permute-done | bytes 131104 | tf_op jit(solution)/shard_map/ppermute | solution.py:40
  28.0 2.0 %collective-permute-start.15 = (bf16[2,2,16,1024]{3,2,1,0:T(8,128)(2,1)S(1)}, bf16[2,2,16,1024]{3,2,1,0:T(8,128)(2,1)S(1)}, u32[]{:S(2)}, u32[]{:S(2)}) collective-permute-start(bf16[2,2,16,1024]{3,2,1,0:T(8,128)(2,1)S(1)} %collective-permute-done.14.refs_1_), channel_id=1, source_target_pairs={{0,32},{4,228},{8,40},{12,236},{16,48},{20,244},{24,56},{28,252},{... | collective-permute-start | bytes 393224 | tf_op jit(solution)/shard_map/ppermute | solution.py:40
  30.0 3.4 %collective-permute-done.15.refs_2_ = bf16[2,2,16,1024]{3,2,1,0:T(8,128)(2,1)S(1)} collective-permute-done((bf16[2,2,16,1024]{3,2,1,0:T(8,128)(2,1)S(1)}, bf16[2,2,16,1024]{3,2,1,0:T(8,128)(2,1)S(1)}, u32[]{:S(2)}, u32[]{:S(2)}) %collective-permute-start.15) | collective-permute-done | bytes 131104 | tf_op jit(solution)/shard_map/ppermute | solution.py:40
  33.4 0.7 collective-permute-start.16
  34.0 0.0 collective-permute-done.8.refs_0_
  34.0 0.8 collective-permute-start.9
  34.8 2.3 %collective-permute-done.16.refs_3_ = bf16[2,2,16,1024]{3,2,1,0:T(8,128)(2,1)S(1)} collective-permute-done((bf16[2,2,16,1024]{3,2,1,0:T(8,128)(2,1)S(1)}, bf16[2,2,16,1024]{3,2,1,0:T(8,128)(2,1)S(1)}, u32[]{:S(2)}, u32[]{:S(2)}) %collective-permute-start.16) | collective-permute-done | bytes 131104 | tf_op jit(solution)/shard_map/ppermute | solution.py:40
  37.2 2.6 %collective-permute-start.17 = (bf16[8,2,16,1024]{3,2,1,0:T(8,128)(2,1)S(1)}, bf16[8,2,16,1024]{3,2,1,0:T(8,128)(2,1)S(1)}, u32[]{:S(2)}, u32[]{:S(2)}) collective-permute-start(bf16[8,2,16,1024]{3,2,1,0:T(8,128)(2,1)S(1)} %pack.15.refs_0_), channel_id=1, source_target_pairs={{0,8},{4,28},{8,0},{12,20},{16,24},{20,12},{24,16},{28,4},{32,40},... | collective-permute-start | bytes 1572872 | tf_op jit(solution)/shard_map/ppermute | solution.py:40
  39.9 0.0 copy-start.2
  39.9 9.5 %collective-permute-start.7 = (bf16[16,1,16,1024]{3,2,1,0:T(8,128)(2,1)S(1)}, bf16[16,1,16,1024]{3,2,1,0:T(8,128)(2,1)S(1)}, u32[]{:S(2)}, u32[]{:S(2)}) collective-permute-start(bf16[16,1,16,1024]{3,2,1,0:T(8,128)(2,1)S(1)} %pack.12.refs_0_), channel_id=1, source_target_pairs={{0,4},{4,0},{8,12},{12,8},{16,20},{20,16},{24,28},{28,24},{32,36},... | collective-permute-start | bytes 1572872 | tf_op jit(solution)/shard_map/ppermute | solution.py:44
  49.4 0.0 collective-permute-done.9.refs_1_
  49.4 1.2 %collective-permute-start.10 = (bf16[16,1,16,1024]{3,2,1,0:T(8,128)(2,1)S(1)}, bf16[16,1,16,1024]{3,2,1,0:T(8,128)(2,1)S(1)}, u32[]{:S(2)}, u32[]{:S(2)}) collective-permute-start(bf16[16,1,16,1024]{3,2,1,0:T(8,128)(2,1)S(1)} %pack.13.refs_2_), channel_id=1, source_target_pairs={{0,4},{4,0},{8,12},{12,8},{16,20},{20,16},{24,28},{28,24},{32,36},... | collective-permute-start | bytes 1572872 | tf_op jit(solution)/shard_map/ppermute | solution.py:44
  50.6 0.0 collective-permute-done.17.refs_1_
  50.7 1.3 %collective-permute-start.18 = (bf16[16,1,16,1024]{3,2,1,0:T(8,128)(2,1)S(1)}, bf16[16,1,16,1024]{3,2,1,0:T(8,128)(2,1)S(1)}, u32[]{:S(2)}, u32[]{:S(2)}) collective-permute-start(bf16[16,1,16,1024]{3,2,1,0:T(8,128)(2,1)S(1)} %pack.16.refs_0_), channel_id=1, source_target_pairs={{0,24},{4,12},{8,16},{12,4},{16,8},{20,28},{24,0},{28,20},{32,56},... | collective-permute-start | bytes 1572872 | tf_op jit(solution)/shard_map/ppermute | solution.py:40
  51.9 10.8 %collective-permute-start = (bf16[32,1024]{1,0:T(8,128)(2,1)S(1)}, bf16[32,1024]{1,0:T(8,128)(2,1)S(1)}, u32[]{:S(2)}, u32[]{:S(2)}) collective-permute-start(bf16[32,1024]{1,0:T(8,128)(2,1)S(1)} %copy-done.6), channel_id=1, source_target_pairs={{0,4},{4,0},{8,12},{12,8},{16,20},{20,16},{24,28},{28,24},{32,36},... | collective-permute-start | bytes 196616 | tf_op jit(solution)/shard_map/ppermute | solution.py:281
  62.7 1.9 %collective-permute-start.1 = (bf16[32,1024]{1,0:T(8,128)(2,1)S(1)}, bf16[32,1024]{1,0:T(8,128)(2,1)S(1)}, u32[]{:S(2)}, u32[]{:S(2)}) collective-permute-start(bf16[32,1024]{1,0:T(8,128)(2,1)S(1)} %copy-done.5), channel_id=1, source_target_pairs={{4,8},{12,16},{20,24},{28,32},{36,40},{44,48},{52,56},{60,64},{68,... | collective-permute-start | bytes 196616 | tf_op jit(solution)/shard_map/ppermute | solution.py:283
  64.7 0.0 collective-permute-done.within
  64.7 3.9 %collective-permute-done.1.across = bf16[32,1024]{1,0:T(8,128)(2,1)S(1)} collective-permute-done((bf16[32,1024]{1,0:T(8,128)(2,1)S(1)}, bf16[32,1024]{1,0:T(8,128)(2,1)S(1)}, u32[]{:S(2)}, u32[]{:S(2)}) %collective-permute-start.1) | collective-permute-done | bytes 65568 | tf_op jit(solution)/shard_map/ppermute | solution.py:283
  68.6 0.9 first.1
  69.5 1.3 %collective-permute-start.11 = (f32[16,128]{1,0:T(8,128)S(1)}, f32[16,128]{1,0:T(8,128)S(1)}, u32[]{:S(2)}, u32[]{:S(2)}) collective-permute-start(f32[16,128]{1,0:T(8,128)S(1)} %get-tuple-element.21.a), channel_id=1, source_target_pairs={{0,1},{1,0},{2,3},{3,2},{4,5},{5,4},{6,7},{7,6},{8,9},{9,8},{10,11... | collective-permute-start | bytes 24584 | tf_op jit(solution)/shard_map/ppermute | solution.py:296
  70.8 1.3 %collective-permute-done.11.b = f32[16,128]{1,0:T(8,128)S(1)} collective-permute-done((f32[16,128]{1,0:T(8,128)S(1)}, f32[16,128]{1,0:T(8,128)S(1)}, u32[]{:S(2)}, u32[]{:S(2)}) %collective-permute-start.11) | collective-permute-done | bytes 8224 | tf_op jit(solution)/shard_map/ppermute | solution.py:296
  72.1 0.0 collective-permute-done.7.refs_1_
  72.1 2.5 %collective-permute-start.12 = (f32[16,128]{1,0:T(8,128)S(1)}, f32[16,128]{1,0:T(8,128)S(1)}, u32[]{:S(2)}, u32[]{:S(2)}) collective-permute-start(f32[16,128]{1,0:T(8,128)S(1)} %add.1.refs_3_), channel_id=1, source_target_pairs={{0,3},{1,2},{2,1},{3,0},{4,7},{5,6},{6,5},{7,4},{8,11},{9,10},{10,... | collective-permute-start | bytes 24584 | tf_op jit(solution)/shard_map/ppermute | solution.py:303
  74.6 0.0 collective-permute-done.10.refs_3_
  74.6 2.7 %shard_map.46.refs_1_ = f32[1088,1024]{1,0:T(8,128)S(1)} custom-call(bf16[1088,1024]{1,0:T(8,128)(2,1)S(1)} %get-tuple-element.19.x_ref.refs_0_, bf16[3,1024]{1,0:T(4,128)(2,1)S(1)} %copy-done.2, bf16[16,1,16,1024]{3,2,1,0:T(8,128)(2,1)S(1)} %pack.12.refs_0_, bf16[16,1,16,1024]{3,2,1,0:T(8,128)(2,1)S(1)} %collective-permute-done.7.refs_1_, ...), custom_call_target="tpu_custom_call" | custom-call | flops 2281701376 | bytes 6684672 | tf_op jit(solution)/shard_map/pallas_call | solution.py:309
  77.3 0.0 collective-permute-done.12.refs_4_
  77.3 2.1 %shard_map.47 = (bf16[1088,1024]{1,0:T(8,128)(2,1)S(1)}, f32[16,128]{1,0:T(8,128)S(1)}) custom-call(bf16[1088,1024]{1,0:T(8,128)(2,1)S(1)} %get-tuple-element.19.x_ref.refs_0_, f32[1088,1024]{1,0:T(8,128)S(1)} %shard_map.46.refs_1_, bf16[3,1024]{1,0:T(4,128)(2,1)S(1)} %copy-done.3, f32[16,128]{1,0:T(8,128)S(1)} %add.1.refs_3_, ...), custom_call_target="tpu_custom_call" | custom-call | flops 570425344 | bytes 8912896 | tf_op jit(solution)/shard_map/pallas_call | solution.py:325
  79.4 0.0 collective-permute-done.18.refs_1_
  79.4 0.1 pack.17.refs_0_
  79.5 0.1 collective-permute-start.19
  79.7 2.1 %collective-permute-start.23 = (bf16[16,1,16,1024]{3,2,1,0:T(8,128)(2,1)S(1)}, bf16[16,1,16,1024]{3,2,1,0:T(8,128)(2,1)S(1)}, u32[]{:S(2)}, u32[]{:S(2)}) collective-permute-start(bf16[16,1,16,1024]{3,2,1,0:T(8,128)(2,1)S(1)} %pack.18.refs_0_), channel_id=1, source_target_pairs={{0,24},{4,12},{8,16},{12,4},{16,8},{20,28},{24,0},{28,20},{32,56},... | collective-permute-start | bytes 1572872 | tf_op jit(solution)/shard_map/ppermute | solution.py:40
  81.8 1.1 %collective-permute-start.21 = (f32[16,128]{1,0:T(8,128)S(1)}, f32[16,128]{1,0:T(8,128)S(1)}, u32[]{:S(2)}, u32[]{:S(2)}) collective-permute-start(f32[16,128]{1,0:T(8,128)S(1)} %get-tuple-element.24.refs_3_), channel_id=1, source_target_pairs={{0,3},{1,2},{2,1},{3,0},{4,7},{5,6},{6,5},{7,4},{8,11},{9,10},{10,... | collective-permute-start | bytes 24584 | tf_op jit(solution)/shard_map/ppermute | solution.py:261
  82.9 2.2 %collective-permute-start.22 = (f32[16,128]{1,0:T(8,128)S(1)}, f32[16,128]{1,0:T(8,128)S(1)}, u32[]{:S(2)}, u32[]{:S(2)}) collective-permute-start(f32[16,128]{1,0:T(8,128)S(1)} %get-tuple-element.24.refs_3_), channel_id=1, source_target_pairs={{0,2},{1,3},{2,0},{3,1},{4,6},{5,7},{6,4},{7,5},{8,10},{9,11},{10,... | collective-permute-start | bytes 24584 | tf_op jit(solution)/shard_map/ppermute | solution.py:261
  85.0 0.0 collective-permute-done.19.refs_1_
  85.0 2.7 %shard_map.48.refs_1_ = f32[1088,1024]{1,0:T(8,128)S(1)} custom-call(bf16[1088,1024]{1,0:T(8,128)(2,1)S(1)} %get-tuple-element.23.x_ref.refs_0_, bf16[3,1024]{1,0:T(4,128)(2,1)S(1)} %copy-done.2, bf16[32,1,16,1024]{3,2,1,0:T(8,128)(2,1)S(1)} %pack.17.refs_0_, bf16[32,1,16,1024]{3,2,1,0:T(8,128)(2,1)S(1)} %collective-permute-done.19.refs_1_), custom_call_target="tpu_custom_call" | custom-call | flops 2281701376 | bytes 6684672 | tf_op jit(solution)/shard_map/pallas_call | solution.py:309
  87.7 0.0 collective-permute-done.20.refs_4_
  87.7 0.0 collective-permute-done.21.refs_5_
  87.7 2.1 %shard_map.49 = (bf16[1088,1024]{1,0:T(8,128)(2,1)S(1)}, f32[16,128]{1,0:T(8,128)S(1)}) custom-call(bf16[1088,1024]{1,0:T(8,128)(2,1)S(1)} %get-tuple-element.23.x_ref.refs_0_, f32[1088,1024]{1,0:T(8,128)S(1)} %shard_map.48.refs_1_, bf16[3,1024]{1,0:T(4,128)(2,1)S(1)} %copy-done.3, f32[16,128]{1,0:T(8,128)S(1)} %get-tuple-element.24.refs_3_, ...), custom_call_target="tpu_custom_call" | custom-call | flops 570425344 | bytes 8912896 | tf_op jit(solution)/shard_map/pallas_call | solution.py:325
  89.9 0.1 pack.19.refs_0_
  90.0 2.1 %collective-permute-start.24 = (bf16[32,1,16,1024]{3,2,1,0:T(8,128)(2,1)S(1)}, bf16[32,1,16,1024]{3,2,1,0:T(8,128)(2,1)S(1)}, u32[]{:S(2)}, u32[]{:S(2)}) collective-permute-start(bf16[32,1,16,1024]{3,2,1,0:T(8,128)(2,1)S(1)} %pack.19.refs_0_), channel_id=1, source_target_pairs={{0,4},{4,0},{8,12},{12,8},{16,20},{20,16},{24,28},{28,24},{32,36},... | collective-permute-start | bytes 3145736 | tf_op jit(solution)/shard_map/ppermute | solution.py:44
  92.0 0.7 collective-permute-start.25
  92.8 1.7 %collective-permute-start.26 = (f32[16,128]{1,0:T(8,128)S(1)}, f32[16,128]{1,0:T(8,128)S(1)}, u32[]{:S(2)}, u32[]{:S(2)}) collective-permute-start(f32[16,128]{1,0:T(8,128)S(1)} %get-tuple-element.27.refs_3_), channel_id=1, source_target_pairs={{0,3},{1,2},{2,1},{3,0},{4,7},{5,6},{6,5},{7,4},{8,11},{9,10},{10,... | collective-permute-start | bytes 24584 | tf_op jit(solution)/shard_map/ppermute | solution.py:261
  94.5 0.8 collective-permute-start.27
  95.3 2.7 %shard_map.50.refs_1_ = f32[1088,1024]{1,0:T(8,128)S(1)} custom-call(bf16[1088,1024]{1,0:T(8,128)(2,1)S(1)} %get-tuple-element.26.x_ref.refs_0_, bf16[3,1024]{1,0:T(4,128)(2,1)S(1)} %copy-done.2, bf16[32,1,16,1024]{3,2,1,0:T(8,128)(2,1)S(1)} %pack.19.refs_0_, bf16[32,1,16,1024]{3,2,1,0:T(8,128)(2,1)S(1)} %collective-permute-done.24.refs_1_), custom_call_target="tpu_custom_call" | custom-call | flops 2281701376 | bytes 6684672 | tf_op jit(solution)/shard_map/pallas_call | solution.py:309
  98.0 0.0 collective-permute-done.26.refs_5_
  98.0 0.5 collective-permute-done.27.refs_6_
  98.5 2.3 %shard_map.51 = bf16[1024,1024]{1,0:T(8,128)(2,1)} custom-call(bf16[1088,1024]{1,0:T(8,128)(2,1)S(1)} %get-tuple-element.26.x_ref.refs_0_, f32[1088,1024]{1,0:T(8,128)S(1)} %shard_map.50.refs_1_, bf16[3,1024]{1,0:T(4,128)(2,1)S(1)} %copy-done.3, f32[16,128]{1,0:T(8,128)S(1)} %get-tuple-element.27.refs_3_, f32[16,128]{1,0:T(8,128)S(1)} %collective-permute-done.25.refs_4_, ...), custom_call_target="tpu_custom_call" | custom-call | flops 570425344 | bytes 8912896 | tf_op jit(solution)/shard_map/pallas_call | solution.py:325
  (25 shorter events, 0.2 us)
Async XLA Ops:
  0.0 18.3 %copy-start.4 = (bf16[3,1,16,1024]{3,2,1,0:T(8,128)(2,1)S(1)}, bf16[3,1,16,1024]{3,2,1,0:T(8,128)(2,1)}, u32[]{:S(2)}) copy-start(bf16[3,1,16,1024]{3,2,1,0:T(8,128)(2,1)} %param.6) | copy-start | bytes 294916
  0.0 6.5 %collective-permute-start.2 = (bf16[1,3,16,1024]{3,2,1,0:T(8,128)(2,1)}, bf16[1,3,16,1024]{3,2,1,0:T(8,128)(2,1)S(1)}, u32[]{:S(2)}, u32[]{:S(2)}) collective-permute-start(bf16[1,3,16,1024]{3,2,1,0:T(8,128)(2,1)} %bitcast.1), channel_id=1, source_target_pairs={{0,8},{4,28},{8,0},{12,20},{16,24},{20,12},{24,16},{28,4},{32,40},... | collective-permute-start | bytes 294920 | tf_op jit(solution)/shard_map/ppermute | solution.py:40
  3.6 4.9 %collective-permute-start.3 = (bf16[1,3,16,1024]{3,2,1,0:T(8,128)(2,1)}, bf16[1,3,16,1024]{3,2,1,0:T(8,128)(2,1)S(1)}, u32[]{:S(2)}, u32[]{:S(2)}) collective-permute-start(bf16[1,3,16,1024]{3,2,1,0:T(8,128)(2,1)} %bitcast.2), channel_id=1, source_target_pairs={{0,24},{4,12},{8,16},{12,4},{16,8},{20,28},{24,0},{28,20},{32,56},... | collective-permute-start | bytes 294920 | tf_op jit(solution)/shard_map/ppermute | solution.py:40
  3.6 5.7 %collective-permute-start.4 = (bf16[1,3,16,1024]{3,2,1,0:T(8,128)(2,1)}, bf16[1,3,16,1024]{3,2,1,0:T(8,128)(2,1)S(1)}, u32[]{:S(2)}, u32[]{:S(2)}) collective-permute-start(bf16[1,3,16,1024]{3,2,1,0:T(8,128)(2,1)} %bitcast.3), channel_id=1, source_target_pairs={{0,16},{4,20},{8,24},{12,28},{16,0},{20,4},{24,8},{28,12},{32,48},... | collective-permute-start | bytes 294920 | tf_op jit(solution)/shard_map/ppermute | solution.py:40
  9.2 0.9 copy-start.1
  10.1 8.0 %collective-permute-start.5 = (bf16[4,1,16,1024]{3,2,1,0:T(8,128)(2,1)S(1)}, bf16[4,1,16,1024]{3,2,1,0:T(8,128)(2,1)S(1)}, u32[]{:S(2)}, u32[]{:S(2)}) collective-permute-start(bf16[4,1,16,1024]{3,2,1,0:T(8,128)(2,1)S(1)} %pack.10.refs_0_), channel_id=1, source_target_pairs={{0,32},{4,228},{8,40},{12,236},{16,48},{20,244},{24,56},{28,252},{... | collective-permute-start | bytes 393224 | tf_op jit(solution)/shard_map/ppermute | solution.py:40
  18.2 6.5 %collective-permute-start.6 = (bf16[8,1,16,1024]{3,2,1,0:T(8,128)(2,1)S(1)}, bf16[8,1,16,1024]{3,2,1,0:T(8,128)(2,1)S(1)}, u32[]{:S(2)}, u32[]{:S(2)}) collective-permute-start(bf16[8,1,16,1024]{3,2,1,0:T(8,128)(2,1)S(1)} %pack.11.refs_0_), channel_id=1, source_target_pairs={{0,224},{4,36},{8,232},{12,44},{16,240},{20,52},{24,248},{28,60},{... | collective-permute-start | bytes 786440 | tf_op jit(solution)/shard_map/ppermute | solution.py:40
  18.3 4.8 %collective-permute-start.13 = (bf16[1,3,16,1024]{3,2,1,0:T(8,128)(2,1)S(1)}, bf16[1,3,16,1024]{3,2,1,0:T(8,128)(2,1)S(1)}, u32[]{:S(2)}, u32[]{:S(2)}) collective-permute-start(bf16[1,3,16,1024]{3,2,1,0:T(8,128)(2,1)S(1)} %bitcast.5), channel_id=1, source_target_pairs={{0,32},{4,228},{8,40},{12,236},{16,48},{20,244},{24,56},{28,252},{... | collective-permute-start | bytes 294920 | tf_op jit(solution)/shard_map/ppermute | solution.py:40
  23.1 28.8 %copy-start.6 = (bf16[32,1024]{1,0:T(8,128)(2,1)S(1)}, bf16[32,1024]{1,0:T(8,128)(2,1)}, u32[]{:S(2)}) copy-start(bf16[32,1024]{1,0:T(8,128)(2,1)} %get-tuple-element.17) | copy-start | bytes 196612
  23.1 39.6 %copy-start.5 = (bf16[32,1024]{1,0:T(8,128)(2,1)S(1)}, bf16[32,1024]{1,0:T(8,128)(2,1)}, u32[]{:S(2)}) copy-start(bf16[32,1024]{1,0:T(8,128)(2,1)} %get-tuple-element.18) | copy-start | bytes 196612
  23.1 45.5 %copy-start = (bf16[1024,1024]{1,0:T(8,128)(2,1)S(1)}, bf16[1024,1024]{1,0:T(8,128)(2,1)}, u32[]{:S(2)}) copy-start(bf16[1024,1024]{1,0:T(8,128)(2,1)} %x.3) | copy-start | bytes 6291460
  23.1 4.9 %collective-permute-start.14 = (bf16[2,2,16,1024]{3,2,1,0:T(8,128)(2,1)S(1)}, bf16[2,2,16,1024]{3,2,1,0:T(8,128)(2,1)S(1)}, u32[]{:S(2)}, u32[]{:S(2)}) collective-permute-start(bf16[2,2,16,1024]{3,2,1,0:T(8,128)(2,1)S(1)} %pack.14.refs_0_), channel_id=1, source_target_pairs={{0,224},{4,36},{8,232},{12,44},{16,240},{20,52},{24,248},{28,60},{... | collective-permute-start | bytes 393224 | tf_op jit(solution)/shard_map/ppermute | solution.py:40
  24.7 9.3 %collective-permute-start.8 = (bf16[8,1,16,1024]{3,2,1,0:T(8,128)(2,1)S(1)}, bf16[8,1,16,1024]{3,2,1,0:T(8,128)(2,1)S(1)}, u32[]{:S(2)}, u32[]{:S(2)}) collective-permute-start(bf16[8,1,16,1024]{3,2,1,0:T(8,128)(2,1)S(1)} %collective-permute-done.6.refs_1_), channel_id=1, source_target_pairs={{0,32},{4,228},{8,40},{12,236},{16,48},{20,244},{24,56},{28,252},{... | collective-permute-start | bytes 786440 | tf_op jit(solution)/shard_map/ppermute | solution.py:40
  28.0 5.3 %collective-permute-start.15 = (bf16[2,2,16,1024]{3,2,1,0:T(8,128)(2,1)S(1)}, bf16[2,2,16,1024]{3,2,1,0:T(8,128)(2,1)S(1)}, u32[]{:S(2)}, u32[]{:S(2)}) collective-permute-start(bf16[2,2,16,1024]{3,2,1,0:T(8,128)(2,1)S(1)} %collective-permute-done.14.refs_1_), channel_id=1, source_target_pairs={{0,32},{4,228},{8,40},{12,236},{16,48},{20,244},{24,56},{28,252},{... | collective-permute-start | bytes 393224 | tf_op jit(solution)/shard_map/ppermute | solution.py:40
  33.4 3.8 %collective-permute-start.16 = (bf16[2,2,16,1024]{3,2,1,0:T(8,128)(2,1)S(1)}, bf16[2,2,16,1024]{3,2,1,0:T(8,128)(2,1)S(1)}, u32[]{:S(2)}, u32[]{:S(2)}) collective-permute-start(bf16[2,2,16,1024]{3,2,1,0:T(8,128)(2,1)S(1)} %collective-permute-done.15.refs_2_), channel_id=1, source_target_pairs={{0,224},{4,36},{8,232},{12,44},{16,240},{20,52},{24,248},{28,60},{... | collective-permute-start | bytes 393224 | tf_op jit(solution)/shard_map/ppermute | solution.py:40
  34.0 15.4 %collective-permute-start.9 = (bf16[8,1,16,1024]{3,2,1,0:T(8,128)(2,1)S(1)}, bf16[8,1,16,1024]{3,2,1,0:T(8,128)(2,1)S(1)}, u32[]{:S(2)}, u32[]{:S(2)}) collective-permute-start(bf16[8,1,16,1024]{3,2,1,0:T(8,128)(2,1)S(1)} %collective-permute-done.8.refs_0_), channel_id=1, source_target_pairs={{0,224},{4,36},{8,232},{12,44},{16,240},{20,52},{24,248},{28,60},{... | collective-permute-start | bytes 786440 | tf_op jit(solution)/shard_map/ppermute | solution.py:40
  37.2 13.4 %collective-permute-start.17 = (bf16[8,2,16,1024]{3,2,1,0:T(8,128)(2,1)S(1)}, bf16[8,2,16,1024]{3,2,1,0:T(8,128)(2,1)S(1)}, u32[]{:S(2)}, u32[]{:S(2)}) collective-permute-start(bf16[8,2,16,1024]{3,2,1,0:T(8,128)(2,1)S(1)} %pack.15.refs_0_), channel_id=1, source_target_pairs={{0,8},{4,28},{8,0},{12,20},{16,24},{20,12},{24,16},{28,4},{32,40},... | collective-permute-start | bytes 1572872 | tf_op jit(solution)/shard_map/ppermute | solution.py:40
  39.9 34.7 %copy-start.2 = (bf16[3,1024]{1,0:T(4,128)(2,1)S(1)}, bf16[3,1024]{1,0:T(4,128)(2,1)}, u32[]{:S(2)}) copy-start(bf16[3,1024]{1,0:T(4,128)(2,1)} %gain_ref.5) | copy-start | bytes 18436
  39.9 32.2 %collective-permute-start.7 = (bf16[16,1,16,1024]{3,2,1,0:T(8,128)(2,1)S(1)}, bf16[16,1,16,1024]{3,2,1,0:T(8,128)(2,1)S(1)}, u32[]{:S(2)}, u32[]{:S(2)}) collective-permute-start(bf16[16,1,16,1024]{3,2,1,0:T(8,128)(2,1)S(1)} %pack.12.refs_0_), channel_id=1, source_target_pairs={{0,4},{4,0},{8,12},{12,8},{16,20},{20,16},{24,28},{28,24},{32,36},... | collective-permute-start | bytes 1572872 | tf_op jit(solution)/shard_map/ppermute | solution.py:44
  49.4 25.1 %collective-permute-start.10 = (bf16[16,1,16,1024]{3,2,1,0:T(8,128)(2,1)S(1)}, bf16[16,1,16,1024]{3,2,1,0:T(8,128)(2,1)S(1)}, u32[]{:S(2)}, u32[]{:S(2)}) collective-permute-start(bf16[16,1,16,1024]{3,2,1,0:T(8,128)(2,1)S(1)} %pack.13.refs_2_), channel_id=1, source_target_pairs={{0,4},{4,0},{8,12},{12,8},{16,20},{20,16},{24,28},{28,24},{32,36},... | collective-permute-start | bytes 1572872 | tf_op jit(solution)/shard_map/ppermute | solution.py:44
  50.7 28.8 %collective-permute-start.18 = (bf16[16,1,16,1024]{3,2,1,0:T(8,128)(2,1)S(1)}, bf16[16,1,16,1024]{3,2,1,0:T(8,128)(2,1)S(1)}, u32[]{:S(2)}, u32[]{:S(2)}) collective-permute-start(bf16[16,1,16,1024]{3,2,1,0:T(8,128)(2,1)S(1)} %pack.16.refs_0_), channel_id=1, source_target_pairs={{0,24},{4,12},{8,16},{12,4},{16,8},{20,28},{24,0},{28,20},{32,56},... | collective-permute-start | bytes 1572872 | tf_op jit(solution)/shard_map/ppermute | solution.py:40
  51.9 12.7 %collective-permute-start = (bf16[32,1024]{1,0:T(8,128)(2,1)S(1)}, bf16[32,1024]{1,0:T(8,128)(2,1)S(1)}, u32[]{:S(2)}, u32[]{:S(2)}) collective-permute-start(bf16[32,1024]{1,0:T(8,128)(2,1)S(1)} %copy-done.6), channel_id=1, source_target_pairs={{0,4},{4,0},{8,12},{12,8},{16,20},{20,16},{24,28},{28,24},{32,36},... | collective-permute-start | bytes 196616 | tf_op jit(solution)/shard_map/ppermute | solution.py:281
  62.7 5.9 %collective-permute-start.1 = (bf16[32,1024]{1,0:T(8,128)(2,1)S(1)}, bf16[32,1024]{1,0:T(8,128)(2,1)S(1)}, u32[]{:S(2)}, u32[]{:S(2)}) collective-permute-start(bf16[32,1024]{1,0:T(8,128)(2,1)S(1)} %copy-done.5), channel_id=1, source_target_pairs={{4,8},{12,16},{20,24},{28,32},{36,40},{44,48},{52,56},{60,64},{68,... | collective-permute-start | bytes 196616 | tf_op jit(solution)/shard_map/ppermute | solution.py:283
  69.5 2.6 %collective-permute-start.11 = (f32[16,128]{1,0:T(8,128)S(1)}, f32[16,128]{1,0:T(8,128)S(1)}, u32[]{:S(2)}, u32[]{:S(2)}) collective-permute-start(f32[16,128]{1,0:T(8,128)S(1)} %get-tuple-element.21.a), channel_id=1, source_target_pairs={{0,1},{1,0},{2,3},{3,2},{4,5},{5,4},{6,7},{7,6},{8,9},{9,8},{10,11... | collective-permute-start | bytes 24584 | tf_op jit(solution)/shard_map/ppermute | solution.py:296
  72.1 5.2 %collective-permute-start.12 = (f32[16,128]{1,0:T(8,128)S(1)}, f32[16,128]{1,0:T(8,128)S(1)}, u32[]{:S(2)}, u32[]{:S(2)}) collective-permute-start(f32[16,128]{1,0:T(8,128)S(1)} %add.1.refs_3_), channel_id=1, source_target_pairs={{0,3},{1,2},{2,1},{3,0},{4,7},{5,6},{6,5},{7,4},{8,11},{9,10},{10,... | collective-permute-start | bytes 24584 | tf_op jit(solution)/shard_map/ppermute | solution.py:303
  74.6 2.7 %copy-start.3 = (bf16[3,1024]{1,0:T(4,128)(2,1)S(1)}, bf16[3,1024]{1,0:T(4,128)(2,1)}, u32[]{:S(2)}) copy-start(bf16[3,1024]{1,0:T(4,128)(2,1)} %refs_2_.5) | copy-start | bytes 18436
  79.5 5.5 %collective-permute-start.19 = (bf16[32,1,16,1024]{3,2,1,0:T(8,128)(2,1)S(1)}, bf16[32,1,16,1024]{3,2,1,0:T(8,128)(2,1)S(1)}, u32[]{:S(2)}, u32[]{:S(2)}) collective-permute-start(bf16[32,1,16,1024]{3,2,1,0:T(8,128)(2,1)S(1)} %pack.17.refs_0_), channel_id=1, source_target_pairs={{0,4},{4,0},{8,12},{12,8},{16,20},{20,16},{24,28},{28,24},{32,36},... | collective-permute-start | bytes 3145736 | tf_op jit(solution)/shard_map/ppermute | solution.py:44
  79.7 10.2 %collective-permute-start.23 = (bf16[16,1,16,1024]{3,2,1,0:T(8,128)(2,1)S(1)}, bf16[16,1,16,1024]{3,2,1,0:T(8,128)(2,1)S(1)}, u32[]{:S(2)}, u32[]{:S(2)}) collective-permute-start(bf16[16,1,16,1024]{3,2,1,0:T(8,128)(2,1)S(1)} %pack.18.refs_0_), channel_id=1, source_target_pairs={{0,24},{4,12},{8,16},{12,4},{16,8},{20,28},{24,0},{28,20},{32,56},... | collective-permute-start | bytes 1572872 | tf_op jit(solution)/shard_map/ppermute | solution.py:40
  81.8 6.0 %collective-permute-start.20 = (f32[16,128]{1,0:T(8,128)S(1)}, f32[16,128]{1,0:T(8,128)S(1)}, u32[]{:S(2)}, u32[]{:S(2)}) collective-permute-start(f32[16,128]{1,0:T(8,128)S(1)} %get-tuple-element.24.refs_3_), channel_id=1, source_target_pairs={{0,1},{1,0},{2,3},{3,2},{4,5},{5,4},{6,7},{7,6},{8,9},{9,8},{10,11... | collective-permute-start | bytes 24584 | tf_op jit(solution)/shard_map/ppermute | solution.py:261
  81.8 6.0 %collective-permute-start.21 = (f32[16,128]{1,0:T(8,128)S(1)}, f32[16,128]{1,0:T(8,128)S(1)}, u32[]{:S(2)}, u32[]{:S(2)}) collective-permute-start(f32[16,128]{1,0:T(8,128)S(1)} %get-tuple-element.24.refs_3_), channel_id=1, source_target_pairs={{0,3},{1,2},{2,1},{3,0},{4,7},{5,6},{6,5},{7,4},{8,11},{9,10},{10,... | collective-permute-start | bytes 24584 | tf_op jit(solution)/shard_map/ppermute | solution.py:261
  82.9 4.9 %collective-permute-start.22 = (f32[16,128]{1,0:T(8,128)S(1)}, f32[16,128]{1,0:T(8,128)S(1)}, u32[]{:S(2)}, u32[]{:S(2)}) collective-permute-start(f32[16,128]{1,0:T(8,128)S(1)} %get-tuple-element.24.refs_3_), channel_id=1, source_target_pairs={{0,2},{1,3},{2,0},{3,1},{4,6},{5,7},{6,4},{7,5},{8,10},{9,11},{10,... | collective-permute-start | bytes 24584 | tf_op jit(solution)/shard_map/ppermute | solution.py:261
  90.0 5.3 %collective-permute-start.24 = (bf16[32,1,16,1024]{3,2,1,0:T(8,128)(2,1)S(1)}, bf16[32,1,16,1024]{3,2,1,0:T(8,128)(2,1)S(1)}, u32[]{:S(2)}, u32[]{:S(2)}) collective-permute-start(bf16[32,1,16,1024]{3,2,1,0:T(8,128)(2,1)S(1)} %pack.19.refs_0_), channel_id=1, source_target_pairs={{0,4},{4,0},{8,12},{12,8},{16,20},{20,16},{24,28},{28,24},{32,36},... | collective-permute-start | bytes 3145736 | tf_op jit(solution)/shard_map/ppermute | solution.py:44
  92.0 6.0 %collective-permute-start.25 = (f32[16,128]{1,0:T(8,128)S(1)}, f32[16,128]{1,0:T(8,128)S(1)}, u32[]{:S(2)}, u32[]{:S(2)}) collective-permute-start(f32[16,128]{1,0:T(8,128)S(1)} %get-tuple-element.27.refs_3_), channel_id=1, source_target_pairs={{0,1},{1,0},{2,3},{3,2},{4,5},{5,4},{6,7},{7,6},{8,9},{9,8},{10,11... | collective-permute-start | bytes 24584 | tf_op jit(solution)/shard_map/ppermute | solution.py:261
  92.8 5.2 %collective-permute-start.26 = (f32[16,128]{1,0:T(8,128)S(1)}, f32[16,128]{1,0:T(8,128)S(1)}, u32[]{:S(2)}, u32[]{:S(2)}) collective-permute-start(f32[16,128]{1,0:T(8,128)S(1)} %get-tuple-element.27.refs_3_), channel_id=1, source_target_pairs={{0,3},{1,2},{2,1},{3,0},{4,7},{5,6},{6,5},{7,4},{8,11},{9,10},{10,... | collective-permute-start | bytes 24584 | tf_op jit(solution)/shard_map/ppermute | solution.py:261
  94.5 4.0 %collective-permute-start.27 = (f32[16,128]{1,0:T(8,128)S(1)}, f32[16,128]{1,0:T(8,128)S(1)}, u32[]{:S(2)}, u32[]{:S(2)}) collective-permute-start(f32[16,128]{1,0:T(8,128)S(1)} %get-tuple-element.27.refs_3_), channel_id=1, source_target_pairs={{0,2},{1,3},{2,0},{3,1},{4,6},{5,7},{6,4},{7,5},{8,10},{9,11},{10,... | collective-permute-start | bytes 24584 | tf_op jit(solution)/shard_map/ppermute | solution.py:261
